TPU v7x, 512 devices: a whole 4x4x16 slice. The times are simulated.
512 devices in a mesh: sp: 16 (over z), fs: 4 (over y), tp: 8 (over x, core).
Axes of the slice: x: 4, y: 4, z: 16, core: 2. Of those that a mesh axis runs over, the one named last changes fastest.
Arguments:
- tokens: bfloat16 [24576, 2048], P(('fs', 'sp', 'tp')), parts along dimension 0, may hold values from -6 to 6
- norm_gain: float32 [2048], replicated, may hold values from 0.1 to 1.9
- w_input: bfloat16 [2048, 1024], P(None, 'tp'), may hold values from -0.125 to 0.125
- w_query: bfloat16 [2048, 1024], P(None, 'tp'), may hold values from -0.125 to 0.125
- w_key: bfloat16 [2048, 1024], P(None, 'tp'), may hold values from -0.125 to 0.125
- w_value: bfloat16 [2048, 1024], P(None, 'tp'), may hold values from -0.125 to 0.125
- query_gain: float32 [64], replicated, may hold values from 0.1 to 1.9
- key_gain: float32 [64], replicated, may hold values from 0.1 to 1.9
- key_bias: bfloat16 [24576, 16], P(('fs', 'sp'), 'tp'), parts along dimension 0, may hold values from -16 to 0
- eigen_real: float32 [64, 64], P('tp'), may hold values from -32 to 0
- eigen_imag: float32 [64, 64], P('tp'), may hold values from 0.31 to 201.0624
- log_step: float32 [64], P('tp'), may hold values from -6.91 to -2.3
- input_real: float32 [64, 64, 16], P('tp'), may hold values from -1 to 1
- input_imag: float32 [64, 64, 16], P('tp'), may hold values from -1 to 1
- read_real: float32 [64, 16, 64], P('tp'), may hold values from -0.75 to 0.75
- read_imag: float32 [64, 16, 64], P('tp'), may hold values from -0.75 to 0.75
- skip_gain: float32 [1024], P('tp'), may hold values from -6 to 6
- w_out_state: bfloat16 [1024, 2048], P('tp'), may hold values from -0.125 to 0.125
- w_out_attn: bfloat16 [1024, 2048], P('tp'), may hold values from -0.125 to 0.125
Outputs:
- layer_out: bfloat16 [24576, 2048], P(('fs', 'sp', 'tp')), parts along dimension 0
There are 4 independent parts, one for each index of `fs`. A program takes and returns all parts, laid end to end along the dimension named above; an argument that names none is the same for every part. Nothing has to cross between parts.
All inputs are finite; a program needn't handle non-finite values.
Results may differ from a plain program's by a relative error of at most 0.014.
Values may be sent and summed in bfloat16 or wider, within the bound.
No kernel may reach another device: no remote copies, remote signals or barrier semaphores. Data moves between devices by JAX's collectives and lax.ppermute only.
A program may use at most 64 MiB of HBM per device.

v0:
```python
import jax
import jax.numpy as jnp
from jax import lax
from jax.experimental import pallas as pl
from jax.experimental.pallas import tpu as pltpu
from jax.sharding import Mesh
from jax.sharding import PartitionSpec as P


GROUP = 16
STATE = 64
HEAD_DIM = 64
TP = ("tp_0", "tp_1")
FS_SP_TP = ("fs", "sp", "tp_0", "tp_1")
EPSILON = 1e-06
F32 = jnp.float32
BF16 = jnp.bfloat16


VMEM = pl.BlockSpec(memory_space=pltpu.VMEM)
SMEM = pl.BlockSpec(memory_space=pltpu.SMEM)


def discretize(eigen_real, eigen_imag, log_step, input_real, input_imag):
    step_size = jnp.exp(log_step)[:, None]
    rotation = eigen_imag * step_size
    shrink = jnp.expm1(eigen_real * step_size)
    cosine = jnp.cos(rotation)
    sine_part = jnp.sin(rotation)
    decay_r = (1.0 + shrink) * cosine
    decay_i = (1.0 + shrink) * sine_part
    minus_r = shrink * cosine - 2.0 * jnp.square(jnp.sin(0.5 * rotation))
    modulus = jnp.square(eigen_real) + jnp.square(eigen_imag)
    factor_r = (minus_r * eigen_real + decay_i * eigen_imag) / modulus
    factor_i = (decay_i * eigen_real - minus_r * eigen_imag) / modulus
    drive_r = factor_r[..., None] * input_real - factor_i[..., None] * input_imag
    drive_i = factor_r[..., None] * input_imag + factor_i[..., None] * input_real
    return (decay_r, decay_i, drive_r, drive_i)


def split(value):
    high = value.astype(BF16)
    low = (value - high.astype(F32)).astype(BF16)
    return high, low


def cmul(ar, ai, br, bi):
    return ar * br - ai * bi, ar * bi + ai * br


def nt_dot(a, b):
    return lax.dot_general(a, b, (((1,), (1,)), ((), ())), preferred_element_type=F32)


def nn_dot(a, b):
    return jnp.dot(a, b, preferred_element_type=F32)


def lanes_low(shape):
    return lax.broadcasted_iota(jnp.int32, shape, len(shape) - 1) < HEAD_DIM


def reorder_matrix(rows, chunks, inverse):
    length = rows // chunks
    r = lax.broadcasted_iota(jnp.int32, (rows, rows), 1 if inverse else 0)
    t = lax.broadcasted_iota(jnp.int32, (rows, rows), 0 if inverse else 1)
    source = (r & (chunks - 1)) * length + (r >> 3)
    return jnp.where(t == source, 1.0, 0.0).astype(BF16)


def norm_kernel(tokens_ref, gain_ref, out_ref):
    wide = tokens_ref[...].astype(F32)
    mean = jnp.sum(wide * wide, axis=1, keepdims=True) * (1.0 / wide.shape[1])
    normed = (wide * lax.rsqrt(mean + EPSILON) * gain_ref[...]).astype(BF16)
    for k in range(out_ref.shape[0]):
        out_ref[k] = normed


def half_project_kernel(mine_ref, w_ref, found_ref):
    found_ref[...] = nn_dot(mine_ref[...], w_ref[...]).astype(BF16)


def merge_kernel(place_ref, parts_ref, mine_ref, other_ref, out_ref, held_ref, sems):
    count = mine_ref.shape[0]
    copies = [
        pltpu.make_async_copy(mine_ref.at[a], held_ref.at[a], sems.at[a]) for a in range(count)
    ]
    for copy in copies:
        copy.start()
    core = place_ref[1]
    total = nn_dot(parts_ref[1 - core], other_ref[0])
    for a in range(1, count):
        total += nn_dot(parts_ref[2 * a + 1 - core], other_ref[a])
    for a in range(count):
        copies[a].wait()
        total += nn_dot(parts_ref[2 * a + core], held_ref[a])
    out_ref[...] = total.astype(BF16)


def block_diagonal(parts, channels, width):
    row = lax.broadcasted_iota(jnp.int32, (channels, width), 0) >> 4
    lane = lax.broadcasted_iota(jnp.int32, (channels, width), 1) >> 6
    return split(jnp.concatenate([jnp.where(row == lane, p, 0.0) for p in parts], axis=1))


def drive_matrices(lines_ref, channels):
    width = lines_ref.shape[1]
    parts = [lines_ref[j * GROUP : (j + 1) * GROUP, :] for j in range(2)]
    parts = [jnp.concatenate([p] * (channels // GROUP), axis=0) for p in parts]
    return block_diagonal(parts, channels, width)


def read_matrices(reads_ref, width):
    channels = reads_ref.shape[0] // 2
    parts = [reads_ref[j * channels : (j + 1) * channels, :] for j in range(2)]
    parts = [jnp.concatenate([p] * (width // 128), axis=1) for p in (parts[0], -parts[1])]
    return block_diagonal(parts, channels, width)


def prepare_kernel(decay_ref, tab_ref, chunk_ref, wide_ref, later_ref, *, blocks, chunk):
    rows = later_ref.shape
    below = lax.broadcasted_iota(jnp.int32, rows, 0) > lax.broadcasted_iota(jnp.int32, rows, 1)
    later_ref[...] = jnp.where(below, 1.0, 0.0).astype(BF16)
    dr, di = decay_ref[0:1, :], decay_ref[1:2, :]
    width = dr.shape[1]
    half = width // 2
    squares = [(dr, di)]
    for _ in range(9):
        a, b = squares[-1]
        squares.append(cmul(a, b, a, b))

    def power(n):
        out = None
        for k in range(10):
            if n >> k & 1:
                out = squares[k] if out is None else cmul(*out, *squares[k])
        return out

    p_chunk = power(chunk)
    p_block = power(chunk * 8)
    now = (jnp.ones_like(dr), jnp.zeros_like(dr))
    for k in range(blocks):
        for j, part in enumerate(now):
            tab_ref[4 * k + 2 * j : 4 * k + 2 * j + 1, :] = part[:, :half]
            tab_ref[4 * k + 2 * j + 1 : 4 * k + 2 * j + 2, :] = part[:, half:]
        now = cmul(*now, *p_block)
    now = (dr, di)
    for c in range(8):
        chunk_ref[c : c + 1, :width] = now[0]
        chunk_ref[c : c + 1, width:] = now[1]
        now = cmul(*now, *p_chunk)
    p2 = cmul(*p_chunk, *p_chunk)
    p4 = cmul(*p2, *p2)
    for k, (a, b) in enumerate([(dr, di), p_chunk, p2, p4]):
        wide_ref[k : k + 1, :width] = a
        wide_ref[k : k + 1, width:] = b
    wide_ref[4:8, :] = jnp.zeros((4, 2 * width), F32)


def make_push(u_perm, b_hi, b_lo, push_ref):
    push_ref[...] = nn_dot(u_perm, b_hi) + nn_dot(u_perm, b_lo)


def project_kernel(
    place_ref, found_ref, other_ref, w_ref, qg_ref, kg_ref, bias_ref, lines_ref, wide_ref,
    q_ref, payload_ref, u_ref, init_ref, rows_ref, push_ref,
):
    rows = payload_ref.shape[0] - 16
    piece = rows // 8
    core = place_ref[1]
    found_other = nn_dot(other_ref[...], w_ref[...]).astype(BF16)
    for found, where in ((found_ref[...], core), (found_other, 1 - core)):
        for a in range(4):
            at = pl.multiple_of((2 * a + where) * piece, 16)
            rows_ref[pl.ds(at, piece), :] = found[a * piece : (a + 1) * piece, :]
    low = lanes_low((rows, 2 * HEAD_DIM))

    def normed(raw, gain):
        wide = raw.astype(F32)
        square = wide * wide
        first = jnp.sum(jnp.where(low, square, 0.0), axis=1, keepdims=True)
        second = jnp.sum(jnp.where(low, 0.0, square), axis=1, keepdims=True)
        scale = jnp.where(
            low,
            lax.rsqrt(first * (1.0 / HEAD_DIM) + EPSILON),
            lax.rsqrt(second * (1.0 / HEAD_DIM) + EPSILON),
        )
        return (wide * scale * gain).astype(BF16)

    u = rows_ref[:, 0:128]
    u_perm = nn_dot(reorder_matrix(rows, 8, False), u).astype(BF16)
    u_ref[...] = u_perm
    make_push(u_perm, *drive_matrices(lines_ref, u_perm.shape[1]), push_ref)
    queries = normed(rows_ref[:, 128:256], qg_ref[...]).astype(F32) * HEAD_DIM ** (-0.5)
    q_ref[0] = jnp.where(low, queries, 0.0).astype(BF16)
    q_ref[1] = jnp.where(low, 0.0, queries).astype(BF16)
    payload_ref[0:rows, 0:128] = normed(rows_ref[:, 256:384], kg_ref[...])
    payload_ref[0:rows, 128:256] = rows_ref[:, 384:512]
    width = push_ref.shape[1] // 2
    lr = jnp.broadcast_to(wide_ref[0:1, :width], (8, width))
    li = jnp.broadcast_to(wide_ref[0:1, width:], (8, width))

    def step(k, carried):
        sr, si = carried
        at = pl.multiple_of(k * 8, 8)
        nr = lr * sr - li * si + push_ref[pl.ds(at, 8), :width]
        ni = lr * si + li * sr + push_ref[pl.ds(at, 8), width:]
        return nr, ni

    zero = jnp.zeros((8, width), F32)
    er, ei = lax.fori_loop(0, piece, step, (zero, zero), unroll=8)
    place = lax.broadcasted_iota(jnp.int32, (8, width), 0)
    for k in range(3):
        shift = 1 << k
        pr, pi = wide_ref[k + 1 : k + 2, :width], wide_ref[k + 1 : k + 2, width:]
        br = jnp.where(place >= shift, pltpu.roll(er, shift, 0), 0.0)
        bi = jnp.where(place >= shift, pltpu.roll(ei, shift, 0), 0.0)
        er, ei = er + pr * br - pi * bi, ei + pr * bi + pi * br
    init_ref[:, :width] = jnp.where(place >= 1, pltpu.roll(er, 1, 0), 0.0)
    init_ref[:, width:] = jnp.where(place >= 1, pltpu.roll(ei, 1, 0), 0.0)
    half = width // 2
    end = [er[7:8, :half], er[7:8, half:], ei[7:8, :half], ei[7:8, half:]]
    highs = [e.astype(BF16).astype(F32) for e in end]
    lows = [e - h for e, h in zip(end, highs)]
    tail = jnp.concatenate([bias_ref[...].astype(F32)] + highs + lows, axis=0)
    payload_ref[rows : rows + 16, :] = tail.astype(BF16)


def read_states(states_ref, ct_hi, ct_lo):
    high, low = split(states_ref[...])
    return nt_dot(high, ct_hi) + nt_dot(low, ct_hi) + nt_dot(high, ct_lo)


def local_state_kernel(
    u_ref, init_ref, lines_ref, wide_ref, reads_ref, skip_ref, y_ref, push_ref
):
    make_push(u_ref[...], *drive_matrices(lines_ref, u_ref.shape[1]), push_ref)
    width = push_ref.shape[1] // 2
    lr = jnp.broadcast_to(wide_ref[0:1, :width], (8, width))
    li = jnp.broadcast_to(wide_ref[0:1, width:], (8, width))

    def step(k, carried):
        sr, si = carried
        at = pl.multiple_of(k * 8, 8)
        nr = lr * sr - li * si + push_ref[pl.ds(at, 8), :width]
        ni = lr * si + li * sr + push_ref[pl.ds(at, 8), width:]
        push_ref[pl.ds(at, 8), :width] = nr
        push_ref[pl.ds(at, 8), width:] = ni
        return nr, ni

    lax.fori_loop(
        0, push_ref.shape[0] // 8, step, (init_ref[:, :width], init_ref[:, width:]), unroll=8
    )
    y_ref[...] = (
        read_states(push_ref, *read_matrices(reads_ref, width))
        + skip_ref[...] * u_ref[...].astype(F32)
    )


def score_block(q_ref, payload_ref, later_ref, diagonal):
    rows = q_ref.shape[1]
    keys, values = payload_ref[0:rows, 0:128], payload_ref[0:rows, 128:256]
    tail = payload_ref[rows : rows + 16, :].astype(F32)
    biases = (
        jnp.concatenate([tail[0:1, :], tail[1:2, 0:128]], axis=1),
        jnp.concatenate([tail[1:2, 128:256], tail[2:3, :]], axis=1),
    )
    outs, totals = [], []
    for h in range(2):
        z = nt_dot(q_ref[h], keys) + biases[h]
        loss = jnp.log(1.0 + jnp.exp(z))
        if diagonal:
            causal = lax.broadcasted_iota(jnp.int32, z.shape, 1) < lax.broadcasted_iota(
                jnp.int32, z.shape, 0
            )
            masked = jnp.where(causal, loss, 0.0)
        else:
            masked = loss
        later = nn_dot(masked.astype(BF16), later_ref[...])
        weights = jnp.exp((z - loss) - later)
        if diagonal:
            weights = jnp.where(causal, weights, 0.0)
        outs.append(nn_dot(weights.astype(BF16), values))
        totals.append(later[:, 0:1] + masked[:, 0:1])
    low = lanes_low((rows, 128))
    return jnp.where(low, outs[0], outs[1]), jnp.where(low, totals[0], totals[1])


def first_kernel(q_ref, payload_ref, later_ref, *refs):
    *state_refs, acc_ref, tot_ref, y_ref, states_ref = refs
    local_state_kernel(*state_refs, y_ref, states_ref)
    out, total = score_block(q_ref, payload_ref, later_ref, True)
    acc_ref[...] = out
    tot_ref[...] = total


def entering_state(payload_ref, tab_ref, carry_ref, power):
    rows = payload_ref.shape[0] - 16
    tail = payload_ref[rows : rows + 16, :].astype(F32)
    er, ei = tail[8:10] + tail[12:14], tail[10:12] + tail[14:16]
    wr, wi = tab_ref[4 * power : 4 * power + 2, :], tab_ref[4 * power + 2 : 4 * power + 4, :]
    carry_ref[0:2, :] += wr * er - wi * ei
    carry_ref[2:4, :] += wr * ei + wi * er


def step_kernel(
    place_ref, q_ref, later_ref, tab_ref, up_ref, down_ref,
    acc_in, tot_in, wrap_in, carry_in, acc_ref, tot_ref, wrap_ref, carry_ref, *, step, blocks, ups,
):
    here = place_ref[0]
    acc_ref[...] = acc_in[...]
    tot_ref[...] = tot_in[...]
    wrap_ref[...] = wrap_in[...]
    carry_ref[...] = carry_in[...]
    if step <= ups:

        @pl.when(here >= step)
        def _():
            out, total = score_block(q_ref, up_ref, later_ref, False)
            acc_ref[...] += out * jnp.exp(-tot_ref[...])
            tot_ref[...] += total
            entering_state(up_ref, tab_ref, carry_ref, step - 1)

    if step < blocks - ups:

        @pl.when(here >= blocks - step)
        def _():
            out, total = score_block(q_ref, down_ref, later_ref, False)
            wrap_ref[...] = wrap_ref[...] * jnp.exp(-total) + out
            entering_state(down_ref, tab_ref, carry_ref, blocks - 1 - step)


def last_kernel(*refs, **sizes):
    ins, (rest, out_ref, acc_ref, tot_ref, wrap_ref, carry_ref, states_ref) = (
        refs[:10],
        (refs[10:14], *refs[14:]),
    )
    step_kernel(*ins, acc_ref, tot_ref, wrap_ref, carry_ref, **sizes)
    finish_kernel(acc_ref, tot_ref, wrap_ref, carry_ref, *rest, out_ref, states_ref)


def finish_kernel(
    acc_ref, tot_ref, wrap_ref, carry_ref, y_ref, chunk_ref, wide_ref, reads_ref,
    out_ref, states_ref,
):
    rows = acc_ref.shape[0]
    width = states_ref.shape[1] // 2
    sr = jnp.concatenate([carry_ref[0:1, :], carry_ref[1:2, :]], axis=1)
    si = jnp.concatenate([carry_ref[2:3, :], carry_ref[3:4, :]], axis=1)
    zr, zi = cmul(chunk_ref[:, :width], chunk_ref[:, width:], sr, si)
    lr = jnp.broadcast_to(wide_ref[0:1, :width], (8, width))
    li = jnp.broadcast_to(wide_ref[0:1, width:], (8, width))

    def step(k, carried):
        zr, zi = carried
        at = pl.multiple_of(k * 8, 8)
        states_ref[pl.ds(at, 8), :width] = zr
        states_ref[pl.ds(at, 8), width:] = zi
        return cmul(lr, li, zr, zi)

    lax.fori_loop(0, rows // 8, step, (zr, zi), unroll=8)
    mixed = y_ref[...] + read_states(states_ref, *read_matrices(reads_ref, width))
    state_out = jax.nn.gelu(mixed).astype(BF16)
    state_out = nn_dot(reorder_matrix(rows, 8, True), state_out).astype(BF16)
    attended = acc_ref[...] + wrap_ref[...] * jnp.exp(-tot_ref[...])
    low = lanes_low(attended.shape)
    square = attended * attended
    first = jnp.sum(jnp.where(low, square, 0.0), axis=1, keepdims=True)
    second = jnp.sum(jnp.where(low, 0.0, square), axis=1, keepdims=True)
    scale = jnp.where(
        low,
        lax.rsqrt(first * (1.0 / HEAD_DIM) + EPSILON),
        lax.rsqrt(second * (1.0 / HEAD_DIM) + EPSILON),
    )
    attn_out = (attended * scale).astype(BF16)
    out_ref[:, 0:128] = state_out
    out_ref[:, 128:256] = attn_out


def call(kernel, outs, args, scratch=(), smem=0, flops=1, aliases={}, limit=16):
    return pl.pallas_call(
        kernel,
        out_shape=outs,
        in_specs=[SMEM] * smem + [VMEM] * (len(args) - smem),
        out_specs=jax.tree.map(lambda _: VMEM, outs),
        scratch_shapes=list(scratch),
        input_output_aliases=aliases,
        compiler_params=pltpu.CompilerParams(vmem_limit_bytes=limit * 2**20),
        cost_estimate=pl.CostEstimate(flops=flops, bytes_accessed=10**6, transcendentals=0),
    )(*args)


def shape(dims, dtype=F32):
    return jax.ShapeDtypeStruct(dims, dtype)


def on_device(
    tokens,
    norm_gain,
    w_input,
    w_query,
    w_key,
    w_value,
    query_gain,
    key_gain,
    key_bias,
    eigen_real,
    eigen_imag,
    log_step,
    input_real,
    input_imag,
    read_real,
    read_imag,
    skip_gain,
    w_out_state,
    w_out_attn,
):
    blocks = lax.axis_size("sp")
    rows = key_bias.shape[0]
    piece = rows // 8
    groups = eigen_real.shape[0]
    width = groups * STATE
    channels = groups * GROUP
    place = jnp.stack([lax.axis_index("sp"), lax.axis_index("tp_1")]).astype(jnp.int32)

    copies = call(
        norm_kernel,
        shape((4, *tokens.shape), BF16),
        (tokens, norm_gain.reshape(1, -1)),
        limit=60,
    )
    mine = lax.all_to_all(copies, "tp_0", 0, 0, tiled=True).reshape(4 * piece, -1)

    w_joined = jnp.concatenate([w_input, w_query, w_key, w_value], axis=1)
    w_out = jnp.concatenate([w_out_state, w_out_attn], axis=0)
    w_out_copies = jnp.broadcast_to(w_out[None], (4, *w_out.shape))
    decay_r, decay_i, drive_r, drive_i = discretize(
        eigen_real, eigen_imag, log_step, input_real, input_imag
    )
    lines = jnp.concatenate(
        [jnp.transpose(part, (2, 0, 1)).reshape(GROUP, width) for part in (drive_r, drive_i)]
    )
    reads = [part.reshape(channels, STATE) for part in (read_real, read_imag)]
    reads = jnp.concatenate([jnp.concatenate([part, part], axis=1) for part in reads])
    decay = jnp.stack([decay_r.reshape(-1), decay_i.reshape(-1)])
    bias8 = jnp.pad(jnp.transpose(key_bias).reshape(-1, 256), ((0, 5), (0, 0)))
    gains = [jnp.tile(g, 2).reshape(1, 128) for g in (query_gain, key_gain)]
    skip = skip_gain.reshape(1, -1)
    decay, lines, reads, w_joined, w_out_copies, bias8, gains, skip, place = (
        lax.optimization_barrier(
            (decay, lines, reads, w_joined, w_out_copies, bias8, gains, skip, place)
        )
    )
    tables = call(
        lambda *refs: prepare_kernel(*refs, blocks=blocks, chunk=piece),
        (
            shape((4 * blocks, width // 2)),
            shape((8, 2 * width)),
            shape((8, 2 * width)),
            shape((rows, rows), BF16),
        ),
        (decay,),
    )
    mine, tables = lax.optimization_barrier((mine, tables))
    tab, chunk, wide, later = tables
    other = lax.ppermute(mine, "tp_1", [(0, 1), (1, 0)])

    found = call(
        half_project_kernel, shape((4 * piece, 512), BF16), (mine, w_joined), flops=10**9
    )
    q, payload, u_perm, init = call(
        project_kernel,
        (
            shape((2, rows, 128), BF16),
            shape((rows + 16, 256), BF16),
            shape((rows, channels), BF16),
            shape((8, 2 * width)),
        ),
        (place, found, other, w_joined, *gains, bias8, lines, wide),
        scratch=(pltpu.VMEM((rows, 512), BF16), pltpu.VMEM((rows, 2 * width), F32)),
        smem=1,
        flops=4 * 10**9,
    )

    u_perm, w_out_copies = lax.optimization_barrier((u_perm, w_out_copies))
    w_out_mine = lax.all_to_all(w_out_copies, "tp_0", 0, 0, tiled=True)
    acc, tot, y_local = call(
        first_kernel,
        (shape((rows, 128)), shape((rows, 128)), shape((rows, channels))),
        (q, payload, later, u_perm, init, lines, wide, reads, skip),
        scratch=(pltpu.VMEM((rows, 2 * width), F32),),
        flops=4 * 10**9,
    )
    wrap = jnp.zeros((rows, 128), F32)
    carry = jnp.zeros((8, width // 2), F32)
    up = down = payload
    half = blocks // 2
    for step in range(1, half + 1):
        up = lax.ppermute(up, "sp", [(i - 1, i) for i in range(step, blocks)])
        if step < half:
            hops = [((j - step + 1) % blocks, (j - step) % blocks) for j in range(half - 1)]
            down = lax.ppermute(down, "sp", hops)
        if step == half:
            break
        acc, tot, wrap, carry = call(
            lambda *refs, step=step: step_kernel(*refs, step=step, blocks=blocks, ups=half),
            (shape((rows, 128)), shape((rows, 128)), shape((rows, 128)), shape(carry.shape)),
            (place, q, later, tab, up, down, acc, tot, wrap, carry),
            smem=1,
            flops=3 * 10**9,
            aliases={6: 0, 7: 1, 8: 2, 9: 3},
        )
        if step == half - 2:
            acc, w_out_mine = lax.optimization_barrier((acc, w_out_mine))
            w_out_other = lax.ppermute(w_out_mine, "tp_1", [(0, 1), (1, 0)])
    state = [shape((rows, 128)), shape((rows, 128)), shape((rows, 128)), shape(carry.shape)]
    both = call(
        lambda *refs: last_kernel(*refs, step=half, blocks=blocks, ups=half),
        shape((rows, 2 * channels), BF16),
        (place, q, later, tab, up, down, acc, tot, wrap, carry, y_local, chunk, wide, reads),
        scratch=[pltpu.VMEM(s.shape, F32) for s in state]
        + [pltpu.VMEM((rows, 2 * width), F32)],
        smem=1,
        flops=3 * 10**9,
    )
    parts = lax.all_to_all(both.reshape(8, piece, -1), TP, 0, 0, tiled=True)
    return pl.pallas_call(
        merge_kernel,
        out_shape=shape((piece, w_out.shape[1]), BF16),
        in_specs=[SMEM, VMEM, pl.BlockSpec(memory_space=pl.ANY), VMEM],
        out_specs=VMEM,
        scratch_shapes=[
            pltpu.VMEM(w_out_mine.shape, BF16),
            pltpu.SemaphoreType.DMA((w_out_mine.shape[0],)),
        ],
        compiler_params=pltpu.CompilerParams(vmem_limit_bytes=16 * 2**20),
        cost_estimate=pl.CostEstimate(flops=10**9, bytes_accessed=10**7, transcendentals=0),
    )(place, parts, w_out_mine, w_out_other)


def solution(mesh):
    torus = Mesh(
        mesh.devices.reshape(mesh.shape["sp"], mesh.shape["fs"], 4, 2), ("sp", "fs", "tp_0", "tp_1")
    )
    placed = (
        P(FS_SP_TP, None),
        P(),
        P(None, TP),
        P(None, TP),
        P(None, TP),
        P(None, TP),
        P(),
        P(),
        P(("fs", "sp"), TP),
        P(TP, None),
        P(TP, None),
        P(TP),
        P(TP, None, None),
        P(TP, None, None),
        P(TP, None, None),
        P(TP, None, None),
        P(TP),
        P(TP, None),
        P(TP, None),
    )

    return jax.shard_map(
        on_device, mesh=torus, in_specs=placed, out_specs=P(FS_SP_TP, None), check_vma=False
    )
```

profile of v0, /device:TPU:408, one launch (start us, length us, event | category | flops | bytes accessed | tf_op | source)
XLA Modules:
  0.0 129.4 jit_solution(8601603489780234856)
XLA Ops:
  0.0 2.0 %shard_map.181 = bf16[4,48,2048]{2,1,0:T(8,128)(2,1)} custom-call(bf16[48,2048]{1,0:T(8,128)(2,1)} %tokens_ref.1, f32[1,2048]{1,0:T(1,128)} %bitcast.19), custom_call_target="tpu_custom_call" | custom-call | flops 1 | bytes 1000000 | tf_op jit(solution)/shard_map/pallas_call | solution.py:381
  2.0 4.3 %all-to-all-start = ((bf16[4,48,2048]{2,1,0:T(8,128)(2,1)}), bf16[4,48,2048]{2,1,0:T(8,128)(2,1)S(1)}, u32[]{:S(2)}, u32[]{:S(2)}) async-start(bf16[4,48,2048]{2,1,0:T(8,128)(2,1)} %shard_map.181), calls=%async_computation | async-start | bytes 1572864 | tf_op jit(solution)/shard_map/all_to_all | solution.py:432
  6.3 0.7 exp.3
  6.9 0.7 tile.4
  7.6 0.1 reshape_tile.6.qg_ref
  7.7 0.7 tile.5
  8.3 0.1 reshape_tile.7.kg_ref
  8.4 0.7 reshape.37
  9.1 0.8 fusion
  9.9 0.1 stack_reshape.7
  10.0 0.1 stack_reshape.6
  10.1 0.9 subtract_bitcast_fusion
  11.0 0.1 reshape.33
  11.1 0.1 reshape.34
  11.2 1.0 maximum_maximum_fusion.refs_4_.refs_13_
  12.3 0.1 pad_add_fusion.place_ref.refs_0_
  12.4 1.3 %pad_maximum_fusion.1 = bf16[256,2048]{1,0:T(8,128)(2,1)S(1)} fusion(bf16[128,2048]{1,0:T(8,128)(2,1)} %param.37, bf16[128,2048]{1,0:T(8,128)(2,1)} %param.36), kind=kLoop, calls=%fused_computation.1 | loop fusion | flops 2097152 | bytes 2097152 | tf_op jit(solution)/shard_map/concatenate | solution.py:435
  13.7 1.7 %pad_maximum_fusion.w_ref = bf16[2048,512]{1,0:T(8,128)(2,1)S(1)} fusion(bf16[2048,128]{1,0:T(8,128)(2,1)} %param.24, bf16[2048,128]{1,0:T(8,128)(2,1)} %param.23, bf16[2048,128]{1,0:T(8,128)(2,1)} %param.22, bf16[2048,128]{1,0:T(8,128)(2,1)} %param.21), kind=kLoop, calls=%fused_computation | loop fusion | flops 8388608 | bytes 4194304 | tf_op jit(solution)/shard_map/concatenate | solution.py:434
  15.4 2.5 %broadcast_in_dim.6 = bf16[4,256,2048]{2,1,0:T(8,128)(2,1)} broadcast(bf16[256,2048]{1,0:T(8,128)(2,1)S(1)} %pad_maximum_fusion.1), dimensions={1,2} | broadcast | bytes 5242880 | tf_op jit(solution)/shard_map/broadcast_in_dim | solution.py:436
  17.9 0.1 shard_map.182
  18.0 0.6 all-to-all-done
  18.6 1.9 %collective-permute-start = (bf16[192,2048]{1,0:T(8,128)(2,1)S(1)}, bf16[192,2048]{1,0:T(8,128)(2,1)S(1)}, u32[]{:S(2)}, u32[]{:S(2)}) collective-permute-start(bf16[192,2048]{1,0:T(8,128)(2,1)S(1)} %bitcast.13), channel_id=1, source_target_pairs={{0,1},{1,0},{2,3},{3,2},{4,5},{5,4},{6,7},{7,6},{8,9},{9,8},{10,11... | collective-permute-start | bytes 2359304 | tf_op jit(solution)/shard_map/ppermute | solution.py:466
  20.5 0.6 shard_map.183.found_ref
  21.1 1.7 %collective-permute-done.other_ref = bf16[192,2048]{1,0:T(8,128)(2,1)S(1)} collective-permute-done((bf16[192,2048]{1,0:T(8,128)(2,1)S(1)}, bf16[192,2048]{1,0:T(8,128)(2,1)S(1)}, u32[]{:S(2)}, u32[]{:S(2)}) %collective-permute-start) | collective-permute-done | bytes 786464 | tf_op jit(solution)/shard_map/ppermute | solution.py:466
  22.7 2.2 %shard_map.184 = (bf16[2,384,128]{2,1,0:T(8,128)(2,1)S(1)}, bf16[400,256]{1,0:T(8,128)(2,1)S(1)}, bf16[384,128]{1,0:T(8,128)(2,1)S(1)}, f32[8,1024]{1,0:T(8,128)S(1)}) custom-call(s32[2]{0:T(128)S(1)} %pad_add_fusion.place_ref.refs_0_, bf16[192,512]{1,0:T(8,128)(2,1)S(1)} %shard_map.183.found_ref, bf16[192,2048]{1,0:T(8,128)(2,1)S(1)} %collective-permute-done.other_ref, ...), custom_call_target="tpu_custom_call" | custom-call | flops 4000000000 | bytes 1000000 | tf_op jit(solution)/shard_map/pallas_call | solution.py:381
  25.0 0.0 copy-start
  25.0 4.9 %all-to-all-start.1 = ((bf16[4,256,2048]{2,1,0:T(8,128)(2,1)}), bf16[4,256,2048]{2,1,0:T(8,128)(2,1)}, u32[]{:S(2)}, u32[]{:S(2)}) async-start(bf16[4,256,2048]{2,1,0:T(8,128)(2,1)} %broadcast_in_dim.6), calls=%async_computation.1 | async-start | bytes 8388608 | tf_op jit(solution)/shard_map/all_to_all | solution.py:486
  29.9 0.7 collective-permute-start.9
  30.6 2.9 %collective-permute-start.1 = (bf16[400,256]{1,0:T(8,128)(2,1)S(1)}, bf16[400,256]{1,0:T(8,128)(2,1)S(1)}, u32[]{:S(2)}, u32[]{:S(2)}) collective-permute-start(bf16[400,256]{1,0:T(8,128)(2,1)S(1)} %get-tuple-element.79.payload_ref), channel_id=1, source_target_pairs={{0,32},{32,64},{64,96},{96,128},{128,160},{160,192},{192,224},{224... | collective-permute-start | bytes 614408 | tf_op jit(solution)/shard_map/ppermute | solution.py:499
  33.5 2.7 %shard_map.185 = (f32[384,128]{1,0:T(8,128)S(1)}, f32[384,128]{1,0:T(8,128)S(1)}, f32[384,128]{1,0:T(8,128)S(1)}) custom-call(bf16[2,384,128]{2,1,0:T(8,128)(2,1)S(1)} %get-tuple-element.76.q_ref.refs_1_, bf16[400,256]{1,0:T(8,128)(2,1)S(1)} %get-tuple-element.79.payload_ref, bf16[384,384]{1,0:T(8,128)(2,1)S(1)} %get-tuple-element.77.later_ref.refs_2_, ...), custom_call_target="tpu_custom_call" | custom-call | flops 4000000000 | bytes 1000000 | tf_op jit(solution)/shard_map/pallas_call | solution.py:381
  36.2 0.0 collective-permute-done.9.refs_5_
  36.2 0.7 collective-permute-start.10
  36.9 3.9 %collective-permute-done.1.refs_4_ = bf16[400,256]{1,0:T(8,128)(2,1)S(1)} collective-permute-done((bf16[400,256]{1,0:T(8,128)(2,1)S(1)}, bf16[400,256]{1,0:T(8,128)(2,1)S(1)}, u32[]{:S(2)}, u32[]{:S(2)}) %collective-permute-start.1) | collective-permute-done | bytes 204832 | tf_op jit(solution)/shard_map/ppermute | solution.py:499
  40.8 1.9 %collective-permute-start.2 = (bf16[400,256]{1,0:T(8,128)(2,1)S(1)}, bf16[400,256]{1,0:T(8,128)(2,1)S(1)}, u32[]{:S(2)}, u32[]{:S(2)}) collective-permute-start(bf16[400,256]{1,0:T(8,128)(2,1)S(1)} %collective-permute-done.1.refs_4_), channel_id=1, source_target_pairs={{32,64},{64,96},{96,128},{128,160},{160,192},{192,224},{224,256},{... | collective-permute-start | bytes 614408 | tf_op jit(solution)/shard_map/ppermute | solution.py:499
  42.8 1.9 %shard_map.186 = (f32[384,128]{1,0:T(8,128)S(1)}, f32[384,128]{1,0:T(8,128)S(1)}, f32[384,128]{1,0:T(8,128)S(1)}, f32[8,256]{1,0:T(8,128)S(1)}) custom-call(s32[2]{0:T(128)S(1)} %pad_add_fusion.place_ref.refs_0_, bf16[2,384,128]{2,1,0:T(8,128)(2,1)S(1)} %get-tuple-element.76.q_ref.refs_1_, ...), custom_call_target="tpu_custom_call", output_to_operand_aliasing={{0}: (6, {}), {1}: (7, {}), {2}: (8, {}), {3}: (9, {})} | custom-call | flops 3000000000 | bytes 1000000 | tf_op jit(solution)/shard_map/pallas_call | solution.py:381
  44.7 0.0 collective-permute-done.10.refs_5_
  44.7 0.7 collective-permute-start.11
  45.4 4.9 %collective-permute-done.2.refs_4_ = bf16[400,256]{1,0:T(8,128)(2,1)S(1)} collective-permute-done((bf16[400,256]{1,0:T(8,128)(2,1)S(1)}, bf16[400,256]{1,0:T(8,128)(2,1)S(1)}, u32[]{:S(2)}, u32[]{:S(2)}) %collective-permute-start.2) | collective-permute-done | bytes 204832 | tf_op jit(solution)/shard_map/ppermute | solution.py:499
  50.3 1.9 %collective-permute-start.3 = (bf16[400,256]{1,0:T(8,128)(2,1)S(1)}, bf16[400,256]{1,0:T(8,128)(2,1)S(1)}, u32[]{:S(2)}, u32[]{:S(2)}) collective-permute-start(bf16[400,256]{1,0:T(8,128)(2,1)S(1)} %collective-permute-done.2.refs_4_), channel_id=1, source_target_pairs={{64,96},{96,128},{128,160},{160,192},{192,224},{224,256},{256,288}... | collective-permute-start | bytes 614408 | tf_op jit(solution)/shard_map/ppermute | solution.py:499
  52.2 1.9 %shard_map.187 = (f32[384,128]{1,0:T(8,128)S(1)}, f32[384,128]{1,0:T(8,128)S(1)}, f32[384,128]{1,0:T(8,128)S(1)}, f32[8,256]{1,0:T(8,128)S(1)}) custom-call(s32[2]{0:T(128)S(1)} %pad_add_fusion.place_ref.refs_0_, bf16[2,384,128]{2,1,0:T(8,128)(2,1)S(1)} %get-tuple-element.76.q_ref.refs_1_, ...), custom_call_target="tpu_custom_call", output_to_operand_aliasing={{0}: (6, {}), {1}: (7, {}), {2}: (8, {}), {3}: (9, {})} | custom-call | flops 3000000000 | bytes 1000000 | tf_op jit(solution)/shard_map/pallas_call | solution.py:381
  54.1 0.0 collective-permute-done.11.refs_5_
  54.1 1.3 collective-permute-start.12
  55.4 3.7 %collective-permute-done.3.refs_4_ = bf16[400,256]{1,0:T(8,128)(2,1)S(1)} collective-permute-done((bf16[400,256]{1,0:T(8,128)(2,1)S(1)}, bf16[400,256]{1,0:T(8,128)(2,1)S(1)}, u32[]{:S(2)}, u32[]{:S(2)}) %collective-permute-start.3) | collective-permute-done | bytes 204832 | tf_op jit(solution)/shard_map/ppermute | solution.py:499
  59.1 1.9 %collective-permute-start.4 = (bf16[400,256]{1,0:T(8,128)(2,1)S(1)}, bf16[400,256]{1,0:T(8,128)(2,1)S(1)}, u32[]{:S(2)}, u32[]{:S(2)}) collective-permute-start(bf16[400,256]{1,0:T(8,128)(2,1)S(1)} %collective-permute-done.3.refs_4_), channel_id=1, source_target_pairs={{96,128},{128,160},{160,192},{192,224},{224,256},{256,288},{288,32... | collective-permute-start | bytes 614408 | tf_op jit(solution)/shard_map/ppermute | solution.py:499
  61.0 2.1 %shard_map.188 = (f32[384,128]{1,0:T(8,128)S(1)}, f32[384,128]{1,0:T(8,128)S(1)}, f32[384,128]{1,0:T(8,128)S(1)}, f32[8,256]{1,0:T(8,128)S(1)}) custom-call(s32[2]{0:T(128)S(1)} %pad_add_fusion.place_ref.refs_0_, bf16[2,384,128]{2,1,0:T(8,128)(2,1)S(1)} %get-tuple-element.76.q_ref.refs_1_, ...), custom_call_target="tpu_custom_call", output_to_operand_aliasing={{0}: (6, {}), {1}: (7, {}), {2}: (8, {}), {3}: (9, {})} | custom-call | flops 3000000000 | bytes 1000000 | tf_op jit(solution)/shard_map/pallas_call | solution.py:381
  63.2 5.2 %collective-permute-start.13 = (bf16[400,256]{1,0:T(8,128)(2,1)S(1)}, bf16[400,256]{1,0:T(8,128)(2,1)S(1)}, u32[]{:S(2)}, u32[]{:S(2)}) collective-permute-start(bf16[400,256]{1,0:T(8,128)(2,1)S(1)} %collective-permute-done.12.refs_5_), channel_id=1, source_target_pairs={{384,352},{416,384},{448,416},{480,448},{0,480},{32,0},{64,32},{38... | collective-permute-start | bytes 614408 | tf_op jit(solution)/shard_map/ppermute | solution.py:502
  68.3 2.5 %collective-permute-start.5 = (bf16[400,256]{1,0:T(8,128)(2,1)S(1)}, bf16[400,256]{1,0:T(8,128)(2,1)S(1)}, u32[]{:S(2)}, u32[]{:S(2)}) collective-permute-start(bf16[400,256]{1,0:T(8,128)(2,1)S(1)} %collective-permute-done.4.refs_4_), channel_id=1, source_target_pairs={{128,160},{160,192},{192,224},{224,256},{256,288},{288,320},{320,3... | collective-permute-start | bytes 614408 | tf_op jit(solution)/shard_map/ppermute | solution.py:499
  70.8 3.2 %shard_map.189 = (f32[384,128]{1,0:T(8,128)S(1)}, f32[384,128]{1,0:T(8,128)S(1)}, f32[384,128]{1,0:T(8,128)S(1)}, f32[8,256]{1,0:T(8,128)S(1)}) custom-call(s32[2]{0:T(128)S(1)} %pad_add_fusion.place_ref.refs_0_, bf16[2,384,128]{2,1,0:T(8,128)(2,1)S(1)} %get-tuple-element.76.q_ref.refs_1_, ...), custom_call_target="tpu_custom_call", output_to_operand_aliasing={{0}: (6, {}), {1}: (7, {}), {2}: (8, {}), {3}: (9, {})} | custom-call | flops 3000000000 | bytes 1000000 | tf_op jit(solution)/shard_map/pallas_call | solution.py:381
  74.1 3.3 %collective-permute-start.14 = (bf16[400,256]{1,0:T(8,128)(2,1)S(1)}, bf16[400,256]{1,0:T(8,128)(2,1)S(1)}, u32[]{:S(2)}, u32[]{:S(2)}) collective-permute-start(bf16[400,256]{1,0:T(8,128)(2,1)S(1)} %collective-permute-done.13.refs_5_), channel_id=1, source_target_pairs={{352,320},{384,352},{416,384},{448,416},{480,448},{0,480},{32,0},{... | collective-permute-start | bytes 614408 | tf_op jit(solution)/shard_map/ppermute | solution.py:502
  77.3 0.0 collective-permute-done.5.refs_4_
  77.3 2.6 %collective-permute-start.6 = (bf16[400,256]{1,0:T(8,128)(2,1)S(1)}, bf16[400,256]{1,0:T(8,128)(2,1)S(1)}, u32[]{:S(2)}, u32[]{:S(2)}) collective-permute-start(bf16[400,256]{1,0:T(8,128)(2,1)S(1)} %collective-permute-done.5.refs_4_), channel_id=1, source_target_pairs={{160,192},{192,224},{224,256},{256,288},{288,320},{320,352},{352,3... | collective-permute-start | bytes 614408 | tf_op jit(solution)/shard_map/ppermute | solution.py:499
  79.9 3.2 %shard_map.190 = (f32[384,128]{1,0:T(8,128)S(1)}, f32[384,128]{1,0:T(8,128)S(1)}, f32[384,128]{1,0:T(8,128)S(1)}, f32[8,256]{1,0:T(8,128)S(1)}) custom-call(s32[2]{0:T(128)S(1)} %pad_add_fusion.place_ref.refs_0_, bf16[2,384,128]{2,1,0:T(8,128)(2,1)S(1)} %get-tuple-element.76.q_ref.refs_1_, ...), custom_call_target="tpu_custom_call", output_to_operand_aliasing={{0}: (6, {}), {1}: (7, {}), {2}: (8, {}), {3}: (9, {})} | custom-call | flops 3000000000 | bytes 1000000 | tf_op jit(solution)/shard_map/pallas_call | solution.py:381
  83.2 3.0 %collective-permute-done.6.refs_4_ = bf16[400,256]{1,0:T(8,128)(2,1)S(1)} collective-permute-done((bf16[400,256]{1,0:T(8,128)(2,1)S(1)}, bf16[400,256]{1,0:T(8,128)(2,1)S(1)}, u32[]{:S(2)}, u32[]{:S(2)}) %collective-permute-start.6) | collective-permute-done | bytes 204832 | tf_op jit(solution)/shard_map/ppermute | solution.py:499
  86.2 3.2 %shard_map.191 = (f32[384,128]{1,0:T(8,128)S(1)}, f32[384,128]{1,0:T(8,128)S(1)}, f32[384,128]{1,0:T(8,128)S(1)}, f32[8,256]{1,0:T(8,128)S(1)}) custom-call(s32[2]{0:T(128)S(1)} %pad_add_fusion.place_ref.refs_0_, bf16[2,384,128]{2,1,0:T(8,128)(2,1)S(1)} %get-tuple-element.76.q_ref.refs_1_, ...), custom_call_target="tpu_custom_call", output_to_operand_aliasing={{0}: (6, {}), {1}: (7, {}), {2}: (8, {}), {3}: (9, {})} | custom-call | flops 3000000000 | bytes 1000000 | tf_op jit(solution)/shard_map/pallas_call | solution.py:381
  89.4 1.9 %collective-permute-start.16 = (bf16[4,256,2048]{2,1,0:T(8,128)(2,1)}, bf16[4,256,2048]{2,1,0:T(8,128)(2,1)S(1)}, u32[]{:S(2)}, u32[]{:S(2)}) collective-permute-start(bf16[4,256,2048]{2,1,0:T(8,128)(2,1)} %all-to-all-done.1.mine_ref), channel_id=1, source_target_pairs={{0,1},{1,0},{2,3},{3,2},{4,5},{5,4},{6,7},{7,6},{8,9},{9,8},{10,11... | collective-permute-start | bytes 12582920 | tf_op jit(solution)/shard_map/ppermute | solution.py:515
  91.4 1.9 %collective-permute-start.7 = (bf16[400,256]{1,0:T(8,128)(2,1)S(1)}, bf16[400,256]{1,0:T(8,128)(2,1)S(1)}, u32[]{:S(2)}, u32[]{:S(2)}) collective-permute-start(bf16[400,256]{1,0:T(8,128)(2,1)S(1)} %collective-permute-done.6.refs_4_), channel_id=1, source_target_pairs={{192,224},{224,256},{256,288},{288,320},{320,352},{352,384},{384,4... | collective-permute-start | bytes 614408 | tf_op jit(solution)/shard_map/ppermute | solution.py:499
  93.3 5.1 %collective-permute-start.15 = (bf16[400,256]{1,0:T(8,128)(2,1)S(1)}, bf16[400,256]{1,0:T(8,128)(2,1)S(1)}, u32[]{:S(2)}, u32[]{:S(2)}) collective-permute-start(bf16[400,256]{1,0:T(8,128)(2,1)S(1)} %collective-permute-done.14.refs_5_), channel_id=1, source_target_pairs={{320,288},{352,320},{384,352},{416,384},{448,416},{480,448},{0,480... | collective-permute-start | bytes 614408 | tf_op jit(solution)/shard_map/ppermute | solution.py:502
  98.4 3.5 %collective-permute-done.7.refs_4_ = bf16[400,256]{1,0:T(8,128)(2,1)S(1)} collective-permute-done((bf16[400,256]{1,0:T(8,128)(2,1)S(1)}, bf16[400,256]{1,0:T(8,128)(2,1)S(1)}, u32[]{:S(2)}, u32[]{:S(2)}) %collective-permute-start.7) | collective-permute-done | bytes 204832 | tf_op jit(solution)/shard_map/ppermute | solution.py:499
  102.0 1.9 %collective-permute-start.8 = (bf16[400,256]{1,0:T(8,128)(2,1)S(1)}, bf16[400,256]{1,0:T(8,128)(2,1)S(1)}, u32[]{:S(2)}, u32[]{:S(2)}) collective-permute-start(bf16[400,256]{1,0:T(8,128)(2,1)S(1)} %collective-permute-done.7.refs_4_), channel_id=1, source_target_pairs={{224,256},{256,288},{288,320},{320,352},{352,384},{384,416},{416,4... | collective-permute-start | bytes 614408 | tf_op jit(solution)/shard_map/ppermute | solution.py:499
  103.9 3.2 %shard_map.192 = (f32[384,128]{1,0:T(8,128)S(1)}, f32[384,128]{1,0:T(8,128)S(1)}, f32[384,128]{1,0:T(8,128)S(1)}, f32[8,256]{1,0:T(8,128)S(1)}) custom-call(s32[2]{0:T(128)S(1)} %pad_add_fusion.place_ref.refs_0_, bf16[2,384,128]{2,1,0:T(8,128)(2,1)S(1)} %get-tuple-element.76.q_ref.refs_1_, ...), custom_call_target="tpu_custom_call", output_to_operand_aliasing={{0}: (6, {}), {1}: (7, {}), {2}: (8, {}), {3}: (9, {})} | custom-call | flops 3000000000 | bytes 1000000 | tf_op jit(solution)/shard_map/pallas_call | solution.py:381
  107.1 4.6 %collective-permute-done.8.refs_4_ = bf16[400,256]{1,0:T(8,128)(2,1)S(1)} collective-permute-done((bf16[400,256]{1,0:T(8,128)(2,1)S(1)}, bf16[400,256]{1,0:T(8,128)(2,1)S(1)}, u32[]{:S(2)}, u32[]{:S(2)}) %collective-permute-start.8) | collective-permute-done | bytes 204832 | tf_op jit(solution)/shard_map/ppermute | solution.py:499
  111.7 3.1 %shard_map.193 = bf16[384,256]{1,0:T(8,128)(2,1)S(1)} custom-call(s32[2]{0:T(128)S(1)} %pad_add_fusion.place_ref.refs_0_, bf16[2,384,128]{2,1,0:T(8,128)(2,1)S(1)} %get-tuple-element.76.q_ref.refs_1_, bf16[384,384]{1,0:T(8,128)(2,1)S(1)} %get-tuple-element.77.later_ref.refs_2_, f32[64,256]{1,0:T(8,128)S(1)} %get-tuple-element.78.refs_3_, ...), custom_call_target="tpu_custom_call" | custom-call | flops 3000000000 | bytes 1000000 | tf_op jit(solution)/shard_map/pallas_call | solution.py:381
  114.8 10.7 %all_to_all.15.parts_ref = bf16[8,48,256]{2,1,0:T(8,128)(2,1)S(1)} all-to-all(bf16[8,48,256]{2,1,0:T(8,128)(2,1)S(1)} %bitcast.15), channel_id=1, replica_groups=mesh['sp'=16,'fs'=4,'tp_0'=4,'tp_1'=2] {'tp_0','tp_1'}, dimensions={0} | all-to-all | bytes 393216 | tf_op jit(solution)/shard_map/all_to_all | solution.py:526
  125.5 3.8 %shard_map.194 = bf16[48,2048]{1,0:T(8,128)(2,1)} custom-call(s32[2]{0:T(128)S(1)} %pad_add_fusion.place_ref.refs_0_, bf16[8,48,256]{2,1,0:T(8,128)(2,1)S(1)} %all_to_all.15.parts_ref, bf16[4,256,2048]{2,1,0:T(8,128)(2,1)} %all-to-all-done.1.mine_ref, bf16[4,256,2048]{2,1,0:T(8,128)(2,1)S(1)} %collective-permute-done.16.other_ref), custom_call_target="tpu_custom_call" | custom-call | flops 1000000000 | bytes 10000000 | tf_op jit(solution)/shard_map/pallas_call | solution.py:527
  (15 shorter events, 0.1 us)
Async XLA Ops:
  2.0 16.6 %all-to-all-start = ((bf16[4,48,2048]{2,1,0:T(8,128)(2,1)}), bf16[4,48,2048]{2,1,0:T(8,128)(2,1)S(1)}, u32[]{:S(2)}, u32[]{:S(2)}) async-start(bf16[4,48,2048]{2,1,0:T(8,128)(2,1)} %shard_map.181), calls=%async_computation | async-start | bytes 1572864 | tf_op jit(solution)/shard_map/all_to_all | solution.py:432
  18.6 4.2 %collective-permute-start = (bf16[192,2048]{1,0:T(8,128)(2,1)S(1)}, bf16[192,2048]{1,0:T(8,128)(2,1)S(1)}, u32[]{:S(2)}, u32[]{:S(2)}) collective-permute-start(bf16[192,2048]{1,0:T(8,128)(2,1)S(1)} %bitcast.13), channel_id=1, source_target_pairs={{0,1},{1,0},{2,3},{3,2},{4,5},{5,4},{6,7},{7,6},{8,9},{9,8},{10,11... | collective-permute-start | bytes 2359304 | tf_op jit(solution)/shard_map/ppermute | solution.py:466
  25.0 8.6 %copy-start = (f32[128]{0:T(128)S(1)}, f32[128]{0:T(128)}, u32[]{:S(2)}) copy-start(f32[128]{0:T(128)} %param.35) | copy-start | bytes 1540
  25.0 64.4 %all-to-all-start.1 = ((bf16[4,256,2048]{2,1,0:T(8,128)(2,1)}), bf16[4,256,2048]{2,1,0:T(8,128)(2,1)}, u32[]{:S(2)}, u32[]{:S(2)}) async-start(bf16[4,256,2048]{2,1,0:T(8,128)(2,1)} %broadcast_in_dim.6), calls=%async_computation.1 | async-start | bytes 8388608 | tf_op jit(solution)/shard_map/all_to_all | solution.py:486
  29.9 6.3 %collective-permute-start.9 = (bf16[400,256]{1,0:T(8,128)(2,1)S(1)}, bf16[400,256]{1,0:T(8,128)(2,1)S(1)}, u32[]{:S(2)}, u32[]{:S(2)}) collective-permute-start(bf16[400,256]{1,0:T(8,128)(2,1)S(1)} %get-tuple-element.79.payload_ref), channel_id=1, source_target_pairs={{0,480},{32,0},{64,32},{96,64},{128,96},{160,128},{192,160},{1,481... | collective-permute-start | bytes 614408 | tf_op jit(solution)/shard_map/ppermute | solution.py:502
  30.6 10.2 %collective-permute-start.1 = (bf16[400,256]{1,0:T(8,128)(2,1)S(1)}, bf16[400,256]{1,0:T(8,128)(2,1)S(1)}, u32[]{:S(2)}, u32[]{:S(2)}) collective-permute-start(bf16[400,256]{1,0:T(8,128)(2,1)S(1)} %get-tuple-element.79.payload_ref), channel_id=1, source_target_pairs={{0,32},{32,64},{64,96},{96,128},{128,160},{160,192},{192,224},{224... | collective-permute-start | bytes 614408 | tf_op jit(solution)/shard_map/ppermute | solution.py:499
  36.2 8.4 %collective-permute-start.10 = (bf16[400,256]{1,0:T(8,128)(2,1)S(1)}, bf16[400,256]{1,0:T(8,128)(2,1)S(1)}, u32[]{:S(2)}, u32[]{:S(2)}) collective-permute-start(bf16[400,256]{1,0:T(8,128)(2,1)S(1)} %collective-permute-done.9.refs_5_), channel_id=1, source_target_pairs={{480,448},{0,480},{32,0},{64,32},{96,64},{128,96},{160,128},{481,4... | collective-permute-start | bytes 614408 | tf_op jit(solution)/shard_map/ppermute | solution.py:502
  40.8 9.5 %collective-permute-start.2 = (bf16[400,256]{1,0:T(8,128)(2,1)S(1)}, bf16[400,256]{1,0:T(8,128)(2,1)S(1)}, u32[]{:S(2)}, u32[]{:S(2)}) collective-permute-start(bf16[400,256]{1,0:T(8,128)(2,1)S(1)} %collective-permute-done.1.refs_4_), channel_id=1, source_target_pairs={{32,64},{64,96},{96,128},{128,160},{160,192},{192,224},{224,256},{... | collective-permute-start | bytes 614408 | tf_op jit(solution)/shard_map/ppermute | solution.py:499
  44.7 9.4 %collective-permute-start.11 = (bf16[400,256]{1,0:T(8,128)(2,1)S(1)}, bf16[400,256]{1,0:T(8,128)(2,1)S(1)}, u32[]{:S(2)}, u32[]{:S(2)}) collective-permute-start(bf16[400,256]{1,0:T(8,128)(2,1)S(1)} %collective-permute-done.10.refs_5_), channel_id=1, source_target_pairs={{448,416},{480,448},{0,480},{32,0},{64,32},{96,64},{128,96},{449,4... | collective-permute-start | bytes 614408 | tf_op jit(solution)/shard_map/ppermute | solution.py:502
  50.3 8.9 %collective-permute-start.3 = (bf16[400,256]{1,0:T(8,128)(2,1)S(1)}, bf16[400,256]{1,0:T(8,128)(2,1)S(1)}, u32[]{:S(2)}, u32[]{:S(2)}) collective-permute-start(bf16[400,256]{1,0:T(8,128)(2,1)S(1)} %collective-permute-done.2.refs_4_), channel_id=1, source_target_pairs={{64,96},{96,128},{128,160},{160,192},{192,224},{224,256},{256,288}... | collective-permute-start | bytes 614408 | tf_op jit(solution)/shard_map/ppermute | solution.py:499
  54.1 9.0 %collective-permute-start.12 = (bf16[400,256]{1,0:T(8,128)(2,1)S(1)}, bf16[400,256]{1,0:T(8,128)(2,1)S(1)}, u32[]{:S(2)}, u32[]{:S(2)}) collective-permute-start(bf16[400,256]{1,0:T(8,128)(2,1)S(1)} %collective-permute-done.11.refs_5_), channel_id=1, source_target_pairs={{416,384},{448,416},{480,448},{0,480},{32,0},{64,32},{96,64},{417,... | collective-permute-start | bytes 614408 | tf_op jit(solution)/shard_map/ppermute | solution.py:502
  59.1 9.2 %collective-permute-start.4 = (bf16[400,256]{1,0:T(8,128)(2,1)S(1)}, bf16[400,256]{1,0:T(8,128)(2,1)S(1)}, u32[]{:S(2)}, u32[]{:S(2)}) collective-permute-start(bf16[400,256]{1,0:T(8,128)(2,1)S(1)} %collective-permute-done.3.refs_4_), channel_id=1, source_target_pairs={{96,128},{128,160},{160,192},{192,224},{224,256},{256,288},{288,32... | collective-permute-start | bytes 614408 | tf_op jit(solution)/shard_map/ppermute | solution.py:499
  63.2 10.9 %collective-permute-start.13 = (bf16[400,256]{1,0:T(8,128)(2,1)S(1)}, bf16[400,256]{1,0:T(8,128)(2,1)S(1)}, u32[]{:S(2)}, u32[]{:S(2)}) collective-permute-start(bf16[400,256]{1,0:T(8,128)(2,1)S(1)} %collective-permute-done.12.refs_5_), channel_id=1, source_target_pairs={{384,352},{416,384},{448,416},{480,448},{0,480},{32,0},{64,32},{38... | collective-permute-start | bytes 614408 | tf_op jit(solution)/shard_map/ppermute | solution.py:502
  68.3 9.0 %collective-permute-start.5 = (bf16[400,256]{1,0:T(8,128)(2,1)S(1)}, bf16[400,256]{1,0:T(8,128)(2,1)S(1)}, u32[]{:S(2)}, u32[]{:S(2)}) collective-permute-start(bf16[400,256]{1,0:T(8,128)(2,1)S(1)} %collective-permute-done.4.refs_4_), channel_id=1, source_target_pairs={{128,160},{160,192},{192,224},{224,256},{256,288},{288,320},{320,3... | collective-permute-start | bytes 614408 | tf_op jit(solution)/shard_map/ppermute | solution.py:499
  74.1 9.1 %collective-permute-start.14 = (bf16[400,256]{1,0:T(8,128)(2,1)S(1)}, bf16[400,256]{1,0:T(8,128)(2,1)S(1)}, u32[]{:S(2)}, u32[]{:S(2)}) collective-permute-start(bf16[400,256]{1,0:T(8,128)(2,1)S(1)} %collective-permute-done.13.refs_5_), channel_id=1, source_target_pairs={{352,320},{384,352},{416,384},{448,416},{480,448},{0,480},{32,0},{... | collective-permute-start | bytes 614408 | tf_op jit(solution)/shard_map/ppermute | solution.py:502
  77.3 8.9 %collective-permute-start.6 = (bf16[400,256]{1,0:T(8,128)(2,1)S(1)}, bf16[400,256]{1,0:T(8,128)(2,1)S(1)}, u32[]{:S(2)}, u32[]{:S(2)}) collective-permute-start(bf16[400,256]{1,0:T(8,128)(2,1)S(1)} %collective-permute-done.5.refs_4_), channel_id=1, source_target_pairs={{160,192},{192,224},{224,256},{256,288},{288,320},{320,352},{352,3... | collective-permute-start | bytes 614408 | tf_op jit(solution)/shard_map/ppermute | solution.py:499
  89.4 36.0 %collective-permute-start.16 = (bf16[4,256,2048]{2,1,0:T(8,128)(2,1)}, bf16[4,256,2048]{2,1,0:T(8,128)(2,1)S(1)}, u32[]{:S(2)}, u32[]{:S(2)}) collective-permute-start(bf16[4,256,2048]{2,1,0:T(8,128)(2,1)} %all-to-all-done.1.mine_ref), channel_id=1, source_target_pairs={{0,1},{1,0},{2,3},{3,2},{4,5},{5,4},{6,7},{7,6},{8,9},{9,8},{10,11... | collective-permute-start | bytes 12582920 | tf_op jit(solution)/shard_map/ppermute | solution.py:515
  91.4 10.6 %collective-permute-start.7 = (bf16[400,256]{1,0:T(8,128)(2,1)S(1)}, bf16[400,256]{1,0:T(8,128)(2,1)S(1)}, u32[]{:S(2)}, u32[]{:S(2)}) collective-permute-start(bf16[400,256]{1,0:T(8,128)(2,1)S(1)} %collective-permute-done.6.refs_4_), channel_id=1, source_target_pairs={{192,224},{224,256},{256,288},{288,320},{320,352},{352,384},{384,4... | collective-permute-start | bytes 614408 | tf_op jit(solution)/shard_map/ppermute | solution.py:499
  93.3 10.6 %collective-permute-start.15 = (bf16[400,256]{1,0:T(8,128)(2,1)S(1)}, bf16[400,256]{1,0:T(8,128)(2,1)S(1)}, u32[]{:S(2)}, u32[]{:S(2)}) collective-permute-start(bf16[400,256]{1,0:T(8,128)(2,1)S(1)} %collective-permute-done.14.refs_5_), channel_id=1, source_target_pairs={{320,288},{352,320},{384,352},{416,384},{448,416},{480,448},{0,480... | collective-permute-start | bytes 614408 | tf_op jit(solution)/shard_map/ppermute | solution.py:502
  102.0 9.7 %collective-permute-start.8 = (bf16[400,256]{1,0:T(8,128)(2,1)S(1)}, bf16[400,256]{1,0:T(8,128)(2,1)S(1)}, u32[]{:S(2)}, u32[]{:S(2)}) collective-permute-start(bf16[400,256]{1,0:T(8,128)(2,1)S(1)} %collective-permute-done.7.refs_4_), channel_id=1, source_target_pairs={{224,256},{256,288},{288,320},{320,352},{352,384},{384,416},{416,4... | collective-permute-start | bytes 614408 | tf_op jit(solution)/shard_map/ppermute | solution.py:499
where the time goes:
time: 130 us; the launch traced here: 129 us
  starting transfers between devices  47.5 us (37%)
  Pallas kernels  33.2 us (26%)
  waiting for transfers between devices  25.9 us (20%)
  blocking collectives  10.7 us (8%)
  other arithmetic  5.89 us (5%)
  local copies, waits for them, and re-layouts  5.71 us (4%)
    pallas_call x13, Pallas kernels, call(): pl.pallas_call(kernel, out_shape=outs, in_specs=[SMEM] * smem + [VMEM] *...  29.4 us
    ppermute x8, waiting for transfers between devices, on_device(): up = lax.ppermute(up, 'sp', [(i - 1, i) for i in range(step, blocks)])  23.7 us
    ppermute x8, starting transfers between devices, on_device(): up = lax.ppermute(up, 'sp', [(i - 1, i) for i in range(step, blocks)])  17.6 us
    ppermute x7, starting transfers between devices, on_device(): down = lax.ppermute(down, 'sp', hops)  16.9 us
    all_to_all x1, blocking collectives, on_device(): parts = lax.all_to_all(both.reshape(8, piece, -1), TP, 0, 0, tiled=True)  10.7 us
    all_to_all x1, starting transfers between devices, on_device(): w_out_mine = lax.all_to_all(w_out_copies, 'tp_0', 0, 0, tiled=True)  4.91 us
    all_to_all x1, starting transfers between devices, on_device(): lax.all_to_all(copies, 'tp_0', 0, 0, tiled=True).reshape(4 * piece, -1)  4.29 us
    pallas_call x1, Pallas kernels, on_device(): pl.pallas_call(merge_kernel, out_shape=shape((piece, w_out.shape[1]), BF1...  3.8 us
  transfers between devices with their start and end apart: 19, of which 8 were waited for; matrix products, arithmetic and copies ran while one was open for 9% of the time, Pallas kernels for 19%

commit v1 on v0

--- a/solution.py
+++ b/solution.py
@@ -286,9 +286,7 @@
     return jnp.where(low, outs[0], outs[1]), jnp.where(low, totals[0], totals[1])
 
 
-def first_kernel(q_ref, payload_ref, later_ref, *refs):
-    *state_refs, acc_ref, tot_ref, y_ref, states_ref = refs
-    local_state_kernel(*state_refs, y_ref, states_ref)
+def first_kernel(q_ref, payload_ref, later_ref, acc_ref, tot_ref):
     out, total = score_block(q_ref, payload_ref, later_ref, True)
     acc_ref[...] = out
     tot_ref[...] = total
@@ -484,12 +482,8 @@
 
     u_perm, w_out_copies = lax.optimization_barrier((u_perm, w_out_copies))
     w_out_mine = lax.all_to_all(w_out_copies, "tp_0", 0, 0, tiled=True)
-    acc, tot, y_local = call(
-        first_kernel,
-        (shape((rows, 128)), shape((rows, 128)), shape((rows, channels))),
-        (q, payload, later, u_perm, init, lines, wide, reads, skip),
-        scratch=(pltpu.VMEM((rows, 2 * width), F32),),
-        flops=4 * 10**9,
+    acc, tot = call(
+        first_kernel, (shape((rows, 128)), shape((rows, 128))), (q, payload, later), flops=2 * 10**9
     )
     wrap = jnp.zeros((rows, 128), F32)
     carry = jnp.zeros((8, width // 2), F32)
@@ -510,9 +504,16 @@
             flops=3 * 10**9,
             aliases={6: 0, 7: 1, 8: 2, 9: 3},
         )
-        if step == half - 2:
-            acc, w_out_mine = lax.optimization_barrier((acc, w_out_mine))
-            w_out_other = lax.ppermute(w_out_mine, "tp_1", [(0, 1), (1, 0)])
+    acc, u_perm = lax.optimization_barrier((acc, u_perm))
+    y_local = call(
+        local_state_kernel,
+        shape((rows, channels)),
+        (u_perm, init, lines, wide, reads, skip),
+        scratch=(pltpu.VMEM((rows, 2 * width), F32),),
+        flops=2 * 10**9,
+    )
+    y_local, w_out_mine = lax.optimization_barrier((y_local, w_out_mine))
+    w_out_other = lax.ppermute(w_out_mine, "tp_1", [(0, 1), (1, 0)])
     state = [shape((rows, 128)), shape((rows, 128)), shape((rows, 128)), shape(carry.shape)]
     both = call(
         lambda *refs: last_kernel(*refs, step=half, blocks=blocks, ups=half),

time: 130 us -> 133 us (1.023)
  the two profiles are of different devices: /device:TPU:408 before, /device:TPU:384 now
where the time goes in v1:
time: 133 us; the launch traced here: 132 us
  starting transfers between devices  46.8 us (35%)
  Pallas kernels  33.5 us (25%)
  waiting for transfers between devices  28.7 us (22%)
  blocking collectives  10.7 us (8%)
  other arithmetic  5.89 us (4%)
  local copies, waits for them, and re-layouts  5.71 us (4%)
    pallas_call x14, Pallas kernels, call(): pl.pallas_call(kernel, out_shape=outs, in_specs=[SMEM] * smem + [VMEM] *...  29.7 us
    ppermute x8, waiting for transfers between devices, on_device(): up = lax.ppermute(up, 'sp', [(i - 1, i) for i in range(step, blocks)])  26.4 us
    ppermute x8, starting transfers between devices, on_device(): up = lax.ppermute(up, 'sp', [(i - 1, i) for i in range(step, blocks)])  17.7 us
    ppermute x7, starting transfers between devices, on_device(): down = lax.ppermute(down, 'sp', hops)  16.1 us
    all_to_all x1, blocking collectives, on_device(): parts = lax.all_to_all(both.reshape(8, piece, -1), TP, 0, 0, tiled=True)  10.7 us
    all_to_all x1, starting transfers between devices, on_device(): w_out_mine = lax.all_to_all(w_out_copies, 'tp_0', 0, 0, tiled=True)  4.91 us
    all_to_all x1, starting transfers between devices, on_device(): lax.all_to_all(copies, 'tp_0', 0, 0, tiled=True).reshape(4 * piece, -1)  4.29 us
    pallas_call x1, Pallas kernels, on_device(): pl.pallas_call(merge_kernel, out_shape=shape((piece, w_out.shape[1]), BF1...  3.8 us
  transfers between devices with their start and end apart: 19, of which 7 were waited for; matrix products, arithmetic and copies ran while one was open for 9% of the time, Pallas kernels for 19%

profile of v1, /device:TPU:384, one launch (start us, length us, event | category | flops | bytes accessed | tf_op | source)
XLA Modules:
  0.0 131.7 jit_solution(8031449388372925763)
XLA Ops:
  0.0 2.0 %shard_map.181 = bf16[4,48,2048]{2,1,0:T(8,128)(2,1)} custom-call(bf16[48,2048]{1,0:T(8,128)(2,1)} %tokens_ref.1, f32[1,2048]{1,0:T(1,128)} %bitcast.19), custom_call_target="tpu_custom_call" | custom-call | flops 1 | bytes 1000000 | tf_op jit(solution)/shard_map/pallas_call | solution.py:379
  2.0 4.3 %all-to-all-start = ((bf16[4,48,2048]{2,1,0:T(8,128)(2,1)}), bf16[4,48,2048]{2,1,0:T(8,128)(2,1)S(1)}, u32[]{:S(2)}, u32[]{:S(2)}) async-start(bf16[4,48,2048]{2,1,0:T(8,128)(2,1)} %shard_map.181), calls=%async_computation | async-start | bytes 1572864 | tf_op jit(solution)/shard_map/all_to_all | solution.py:430
  6.3 0.7 exp.3
  6.9 0.7 tile.4
  7.6 0.1 reshape_tile.6.qg_ref
  7.7 0.7 tile.5
  8.3 0.1 reshape_tile.7.kg_ref
  8.4 0.7 reshape.37
  9.1 0.8 fusion
  9.9 0.1 stack_reshape.7
  10.0 0.1 stack_reshape.6
  10.1 0.9 subtract_bitcast_fusion
  11.0 0.1 reshape.33
  11.1 0.1 reshape.34
  11.2 1.0 maximum_maximum_fusion.reads_ref.refs_13_
  12.3 0.1 pad_add_fusion.place_ref.refs_0_
  12.4 1.3 pad_maximum_fusion.1
  13.7 1.7 %pad_maximum_fusion.w_ref = bf16[2048,512]{1,0:T(8,128)(2,1)S(1)} fusion(bf16[2048,128]{1,0:T(8,128)(2,1)} %param.24, bf16[2048,128]{1,0:T(8,128)(2,1)} %param.23, bf16[2048,128]{1,0:T(8,128)(2,1)} %param.22, bf16[2048,128]{1,0:T(8,128)(2,1)} %param.21), kind=kLoop, calls=%fused_computation | loop fusion | flops 8388608 | bytes 4194304 | tf_op jit(solution)/shard_map/concatenate | solution.py:432
  15.4 2.5 %broadcast_in_dim.6 = bf16[4,256,2048]{2,1,0:T(8,128)(2,1)} broadcast(bf16[256,2048]{1,0:T(8,128)(2,1)S(1)} %pad_maximum_fusion.1), dimensions={1,2} | broadcast | bytes 5242880 | tf_op jit(solution)/shard_map/broadcast_in_dim | solution.py:434
  17.9 0.1 shard_map.182
  18.0 0.6 all-to-all-done
  18.6 1.9 %collective-permute-start = (bf16[192,2048]{1,0:T(8,128)(2,1)S(1)}, bf16[192,2048]{1,0:T(8,128)(2,1)S(1)}, u32[]{:S(2)}, u32[]{:S(2)}) collective-permute-start(bf16[192,2048]{1,0:T(8,128)(2,1)S(1)} %bitcast.13), channel_id=1, source_target_pairs={{0,1},{1,0},{2,3},{3,2},{4,5},{5,4},{6,7},{7,6},{8,9},{9,8},{10,11... | collective-permute-start | bytes 2359304 | tf_op jit(solution)/shard_map/ppermute | solution.py:464
  20.5 0.6 shard_map.183.found_ref
  21.1 1.7 %collective-permute-done.other_ref = bf16[192,2048]{1,0:T(8,128)(2,1)S(1)} collective-permute-done((bf16[192,2048]{1,0:T(8,128)(2,1)S(1)}, bf16[192,2048]{1,0:T(8,128)(2,1)S(1)}, u32[]{:S(2)}, u32[]{:S(2)}) %collective-permute-start) | collective-permute-done | bytes 786464 | tf_op jit(solution)/shard_map/ppermute | solution.py:464
  22.7 2.2 %shard_map.184 = (bf16[2,384,128]{2,1,0:T(8,128)(2,1)S(1)}, bf16[400,256]{1,0:T(8,128)(2,1)S(1)}, bf16[384,128]{1,0:T(8,128)(2,1)S(1)}, f32[8,1024]{1,0:T(8,128)S(1)}) custom-call(s32[2]{0:T(128)S(1)} %pad_add_fusion.place_ref.refs_0_, bf16[192,512]{1,0:T(8,128)(2,1)S(1)} %shard_map.183.found_ref, bf16[192,2048]{1,0:T(8,128)(2,1)S(1)} %collective-permute-done.other_ref, ...), custom_call_target="tpu_custom_call" | custom-call | flops 4000000000 | bytes 1000000 | tf_op jit(solution)/shard_map/pallas_call | solution.py:379
  25.0 4.9 %all-to-all-start.1 = ((bf16[4,256,2048]{2,1,0:T(8,128)(2,1)}), bf16[4,256,2048]{2,1,0:T(8,128)(2,1)}, u32[]{:S(2)}, u32[]{:S(2)}) async-start(bf16[4,256,2048]{2,1,0:T(8,128)(2,1)} %broadcast_in_dim.6), calls=%async_computation.1 | async-start | bytes 8388608 | tf_op jit(solution)/shard_map/all_to_all | solution.py:484
  29.9 0.7 collective-permute-start.9
  30.6 2.9 %collective-permute-start.1 = (bf16[400,256]{1,0:T(8,128)(2,1)S(1)}, bf16[400,256]{1,0:T(8,128)(2,1)S(1)}, u32[]{:S(2)}, u32[]{:S(2)}) collective-permute-start(bf16[400,256]{1,0:T(8,128)(2,1)S(1)} %get-tuple-element.80.payload_ref), channel_id=1, source_target_pairs={{0,32},{32,64},{64,96},{96,128},{128,160},{160,192},{192,224},{224... | collective-permute-start | bytes 614408 | tf_op jit(solution)/shard_map/ppermute | solution.py:493
  33.5 1.2 shard_map.185
  34.7 0.0 collective-permute-done.9.refs_5_
  34.7 0.7 collective-permute-start.10
  35.4 5.4 %collective-permute-done.1.refs_4_ = bf16[400,256]{1,0:T(8,128)(2,1)S(1)} collective-permute-done((bf16[400,256]{1,0:T(8,128)(2,1)S(1)}, bf16[400,256]{1,0:T(8,128)(2,1)S(1)}, u32[]{:S(2)}, u32[]{:S(2)}) %collective-permute-start.1) | collective-permute-done | bytes 204832 | tf_op jit(solution)/shard_map/ppermute | solution.py:493
  40.8 1.9 %collective-permute-start.2 = (bf16[400,256]{1,0:T(8,128)(2,1)S(1)}, bf16[400,256]{1,0:T(8,128)(2,1)S(1)}, u32[]{:S(2)}, u32[]{:S(2)}) collective-permute-start(bf16[400,256]{1,0:T(8,128)(2,1)S(1)} %collective-permute-done.1.refs_4_), channel_id=1, source_target_pairs={{32,64},{64,96},{96,128},{128,160},{160,192},{192,224},{224,256},{... | collective-permute-start | bytes 614408 | tf_op jit(solution)/shard_map/ppermute | solution.py:493
  42.7 1.9 %shard_map.186 = (f32[384,128]{1,0:T(8,128)S(1)}, f32[384,128]{1,0:T(8,128)S(1)}, f32[384,128]{1,0:T(8,128)S(1)}, f32[8,256]{1,0:T(8,128)S(1)}) custom-call(s32[2]{0:T(128)S(1)} %pad_add_fusion.place_ref.refs_0_, bf16[2,384,128]{2,1,0:T(8,128)(2,1)S(1)} %get-tuple-element.77.q_ref.refs_1_, ...), custom_call_target="tpu_custom_call", output_to_operand_aliasing={{0}: (6, {}), {1}: (7, {}), {2}: (8, {}), {3}: (9, {})} | custom-call | flops 3000000000 | bytes 1000000 | tf_op jit(solution)/shard_map/pallas_call | solution.py:379
  44.7 0.0 collective-permute-done.10.refs_5_
  44.7 0.7 collective-permute-start.11
  45.4 4.9 %collective-permute-done.2.refs_4_ = bf16[400,256]{1,0:T(8,128)(2,1)S(1)} collective-permute-done((bf16[400,256]{1,0:T(8,128)(2,1)S(1)}, bf16[400,256]{1,0:T(8,128)(2,1)S(1)}, u32[]{:S(2)}, u32[]{:S(2)}) %collective-permute-start.2) | collective-permute-done | bytes 204832 | tf_op jit(solution)/shard_map/ppermute | solution.py:493
  50.3 1.9 %collective-permute-start.3 = (bf16[400,256]{1,0:T(8,128)(2,1)S(1)}, bf16[400,256]{1,0:T(8,128)(2,1)S(1)}, u32[]{:S(2)}, u32[]{:S(2)}) collective-permute-start(bf16[400,256]{1,0:T(8,128)(2,1)S(1)} %collective-permute-done.2.refs_4_), channel_id=1, source_target_pairs={{64,96},{96,128},{128,160},{160,192},{192,224},{224,256},{256,288}... | collective-permute-start | bytes 614408 | tf_op jit(solution)/shard_map/ppermute | solution.py:493
  52.2 1.9 %shard_map.187 = (f32[384,128]{1,0:T(8,128)S(1)}, f32[384,128]{1,0:T(8,128)S(1)}, f32[384,128]{1,0:T(8,128)S(1)}, f32[8,256]{1,0:T(8,128)S(1)}) custom-call(s32[2]{0:T(128)S(1)} %pad_add_fusion.place_ref.refs_0_, bf16[2,384,128]{2,1,0:T(8,128)(2,1)S(1)} %get-tuple-element.77.q_ref.refs_1_, ...), custom_call_target="tpu_custom_call", output_to_operand_aliasing={{0}: (6, {}), {1}: (7, {}), {2}: (8, {}), {3}: (9, {})} | custom-call | flops 3000000000 | bytes 1000000 | tf_op jit(solution)/shard_map/pallas_call | solution.py:379
  54.1 1.3 collective-permute-start.12
  55.4 3.7 %collective-permute-done.3.refs_4_ = bf16[400,256]{1,0:T(8,128)(2,1)S(1)} collective-permute-done((bf16[400,256]{1,0:T(8,128)(2,1)S(1)}, bf16[400,256]{1,0:T(8,128)(2,1)S(1)}, u32[]{:S(2)}, u32[]{:S(2)}) %collective-permute-start.3) | collective-permute-done | bytes 204832 | tf_op jit(solution)/shard_map/ppermute | solution.py:493
  59.1 1.9 %collective-permute-start.4 = (bf16[400,256]{1,0:T(8,128)(2,1)S(1)}, bf16[400,256]{1,0:T(8,128)(2,1)S(1)}, u32[]{:S(2)}, u32[]{:S(2)}) collective-permute-start(bf16[400,256]{1,0:T(8,128)(2,1)S(1)} %collective-permute-done.3.refs_4_), channel_id=1, source_target_pairs={{96,128},{128,160},{160,192},{192,224},{224,256},{256,288},{288,32... | collective-permute-start | bytes 614408 | tf_op jit(solution)/shard_map/ppermute | solution.py:493
  61.0 1.9 %shard_map.188 = (f32[384,128]{1,0:T(8,128)S(1)}, f32[384,128]{1,0:T(8,128)S(1)}, f32[384,128]{1,0:T(8,128)S(1)}, f32[8,256]{1,0:T(8,128)S(1)}) custom-call(s32[2]{0:T(128)S(1)} %pad_add_fusion.place_ref.refs_0_, bf16[2,384,128]{2,1,0:T(8,128)(2,1)S(1)} %get-tuple-element.77.q_ref.refs_1_, ...), custom_call_target="tpu_custom_call", output_to_operand_aliasing={{0}: (6, {}), {1}: (7, {}), {2}: (8, {}), {3}: (9, {})} | custom-call | flops 3000000000 | bytes 1000000 | tf_op jit(solution)/shard_map/pallas_call | solution.py:379
  63.0 5.1 %collective-permute-start.13 = (bf16[400,256]{1,0:T(8,128)(2,1)S(1)}, bf16[400,256]{1,0:T(8,128)(2,1)S(1)}, u32[]{:S(2)}, u32[]{:S(2)}) collective-permute-start(bf16[400,256]{1,0:T(8,128)(2,1)S(1)} %collective-permute-done.12.refs_5_), channel_id=1, source_target_pairs={{384,352},{416,384},{448,416},{480,448},{0,480},{32,0},{64,32},{38... | collective-permute-start | bytes 614408 | tf_op jit(solution)/shard_map/ppermute | solution.py:496
  68.1 2.5 %collective-permute-start.5 = (bf16[400,256]{1,0:T(8,128)(2,1)S(1)}, bf16[400,256]{1,0:T(8,128)(2,1)S(1)}, u32[]{:S(2)}, u32[]{:S(2)}) collective-permute-start(bf16[400,256]{1,0:T(8,128)(2,1)S(1)} %collective-permute-done.4.refs_4_), channel_id=1, source_target_pairs={{128,160},{160,192},{192,224},{224,256},{256,288},{288,320},{320,3... | collective-permute-start | bytes 614408 | tf_op jit(solution)/shard_map/ppermute | solution.py:493
  70.7 3.4 %shard_map.189 = (f32[384,128]{1,0:T(8,128)S(1)}, f32[384,128]{1,0:T(8,128)S(1)}, f32[384,128]{1,0:T(8,128)S(1)}, f32[8,256]{1,0:T(8,128)S(1)}) custom-call(s32[2]{0:T(128)S(1)} %pad_add_fusion.place_ref.refs_0_, bf16[2,384,128]{2,1,0:T(8,128)(2,1)S(1)} %get-tuple-element.77.q_ref.refs_1_, ...), custom_call_target="tpu_custom_call", output_to_operand_aliasing={{0}: (6, {}), {1}: (7, {}), {2}: (8, {}), {3}: (9, {})} | custom-call | flops 3000000000 | bytes 1000000 | tf_op jit(solution)/shard_map/pallas_call | solution.py:379
  74.1 0.0 collective-permute-done.13.refs_5_
  74.1 3.2 %collective-permute-start.14 = (bf16[400,256]{1,0:T(8,128)(2,1)S(1)}, bf16[400,256]{1,0:T(8,128)(2,1)S(1)}, u32[]{:S(2)}, u32[]{:S(2)}) collective-permute-start(bf16[400,256]{1,0:T(8,128)(2,1)S(1)} %collective-permute-done.13.refs_5_), channel_id=1, source_target_pairs={{352,320},{384,352},{416,384},{448,416},{480,448},{0,480},{32,0},{... | collective-permute-start | bytes 614408 | tf_op jit(solution)/shard_map/ppermute | solution.py:496
  77.3 0.0 collective-permute-done.5.refs_4_
  77.3 2.6 %collective-permute-start.6 = (bf16[400,256]{1,0:T(8,128)(2,1)S(1)}, bf16[400,256]{1,0:T(8,128)(2,1)S(1)}, u32[]{:S(2)}, u32[]{:S(2)}) collective-permute-start(bf16[400,256]{1,0:T(8,128)(2,1)S(1)} %collective-permute-done.5.refs_4_), channel_id=1, source_target_pairs={{160,192},{192,224},{224,256},{256,288},{288,320},{320,352},{352,3... | collective-permute-start | bytes 614408 | tf_op jit(solution)/shard_map/ppermute | solution.py:493
  79.9 3.2 %shard_map.190 = (f32[384,128]{1,0:T(8,128)S(1)}, f32[384,128]{1,0:T(8,128)S(1)}, f32[384,128]{1,0:T(8,128)S(1)}, f32[8,256]{1,0:T(8,128)S(1)}) custom-call(s32[2]{0:T(128)S(1)} %pad_add_fusion.place_ref.refs_0_, bf16[2,384,128]{2,1,0:T(8,128)(2,1)S(1)} %get-tuple-element.77.q_ref.refs_1_, ...), custom_call_target="tpu_custom_call", output_to_operand_aliasing={{0}: (6, {}), {1}: (7, {}), {2}: (8, {}), {3}: (9, {})} | custom-call | flops 3000000000 | bytes 1000000 | tf_op jit(solution)/shard_map/pallas_call | solution.py:379
  83.2 0.0 collective-permute-done.14.refs_5_
  83.2 4.4 %collective-permute-start.15 = (bf16[400,256]{1,0:T(8,128)(2,1)S(1)}, bf16[400,256]{1,0:T(8,128)(2,1)S(1)}, u32[]{:S(2)}, u32[]{:S(2)}) collective-permute-start(bf16[400,256]{1,0:T(8,128)(2,1)S(1)} %collective-permute-done.14.refs_5_), channel_id=1, source_target_pairs={{320,288},{352,320},{384,352},{416,384},{448,416},{480,448},{0,480... | collective-permute-start | bytes 614408 | tf_op jit(solution)/shard_map/ppermute | solution.py:496
  87.6 1.9 %collective-permute-start.7 = (bf16[400,256]{1,0:T(8,128)(2,1)S(1)}, bf16[400,256]{1,0:T(8,128)(2,1)S(1)}, u32[]{:S(2)}, u32[]{:S(2)}) collective-permute-start(bf16[400,256]{1,0:T(8,128)(2,1)S(1)} %collective-permute-done.6.refs_4_), channel_id=1, source_target_pairs={{192,224},{224,256},{256,288},{288,320},{320,352},{352,384},{384,4... | collective-permute-start | bytes 614408 | tf_op jit(solution)/shard_map/ppermute | solution.py:493
  89.5 3.2 %shard_map.191 = (f32[384,128]{1,0:T(8,128)S(1)}, f32[384,128]{1,0:T(8,128)S(1)}, f32[384,128]{1,0:T(8,128)S(1)}, f32[8,256]{1,0:T(8,128)S(1)}) custom-call(s32[2]{0:T(128)S(1)} %pad_add_fusion.place_ref.refs_0_, bf16[2,384,128]{2,1,0:T(8,128)(2,1)S(1)} %get-tuple-element.77.q_ref.refs_1_, ...), custom_call_target="tpu_custom_call", output_to_operand_aliasing={{0}: (6, {}), {1}: (7, {}), {2}: (8, {}), {3}: (9, {})} | custom-call | flops 3000000000 | bytes 1000000 | tf_op jit(solution)/shard_map/pallas_call | solution.py:379
  92.8 3.7 %collective-permute-done.7.refs_4_ = bf16[400,256]{1,0:T(8,128)(2,1)S(1)} collective-permute-done((bf16[400,256]{1,0:T(8,128)(2,1)S(1)}, bf16[400,256]{1,0:T(8,128)(2,1)S(1)}, u32[]{:S(2)}, u32[]{:S(2)}) %collective-permute-start.7) | collective-permute-done | bytes 204832 | tf_op jit(solution)/shard_map/ppermute | solution.py:493
  96.5 3.2 %shard_map.192 = (f32[384,128]{1,0:T(8,128)S(1)}, f32[384,128]{1,0:T(8,128)S(1)}, f32[384,128]{1,0:T(8,128)S(1)}, f32[8,256]{1,0:T(8,128)S(1)}) custom-call(s32[2]{0:T(128)S(1)} %pad_add_fusion.place_ref.refs_0_, bf16[2,384,128]{2,1,0:T(8,128)(2,1)S(1)} %get-tuple-element.77.q_ref.refs_1_, ...), custom_call_target="tpu_custom_call", output_to_operand_aliasing={{0}: (6, {}), {1}: (7, {}), {2}: (8, {}), {3}: (9, {})} | custom-call | flops 3000000000 | bytes 1000000 | tf_op jit(solution)/shard_map/pallas_call | solution.py:379
  99.7 1.7 %shard_map.193.refs_10_ = f32[384,128]{1,0:T(8,128)S(1)} custom-call(bf16[384,128]{1,0:T(8,128)(2,1)S(1)} %get-tuple-element.115.u_ref, f32[8,1024]{1,0:T(8,128)S(1)} %get-tuple-element.116.init_ref, f32[32,512]{1,0:T(8,128)S(1)} %pad_maximum_fusion.2.lines_ref, f32[8,1024]{1,0:T(8,128)S(1)} %get-tuple-element.76.wide_ref.refs_12_, ...), custom_call_target="tpu_custom_call" | custom-call | flops 2000000000 | bytes 1000000 | tf_op jit(solution)/shard_map/pallas_call | solution.py:379
  101.4 1.9 %collective-permute-start.16 = (bf16[4,256,2048]{2,1,0:T(8,128)(2,1)}, bf16[4,256,2048]{2,1,0:T(8,128)(2,1)S(1)}, u32[]{:S(2)}, u32[]{:S(2)}) collective-permute-start(bf16[4,256,2048]{2,1,0:T(8,128)(2,1)} %all-to-all-done.1.mine_ref), channel_id=1, source_target_pairs={{0,1},{1,0},{2,3},{3,2},{4,5},{5,4},{6,7},{7,6},{8,9},{9,8},{10,11... | collective-permute-start | bytes 12582920 | tf_op jit(solution)/shard_map/ppermute | solution.py:516
  103.4 1.9 %collective-permute-start.8 = (bf16[400,256]{1,0:T(8,128)(2,1)S(1)}, bf16[400,256]{1,0:T(8,128)(2,1)S(1)}, u32[]{:S(2)}, u32[]{:S(2)}) collective-permute-start(bf16[400,256]{1,0:T(8,128)(2,1)S(1)} %collective-permute-done.7.refs_4_), channel_id=1, source_target_pairs={{224,256},{256,288},{288,320},{320,352},{352,384},{384,416},{416,4... | collective-permute-start | bytes 614408 | tf_op jit(solution)/shard_map/ppermute | solution.py:493
  105.3 8.7 %collective-permute-done.8.refs_4_ = bf16[400,256]{1,0:T(8,128)(2,1)S(1)} collective-permute-done((bf16[400,256]{1,0:T(8,128)(2,1)S(1)}, bf16[400,256]{1,0:T(8,128)(2,1)S(1)}, u32[]{:S(2)}, u32[]{:S(2)}) %collective-permute-start.8) | collective-permute-done | bytes 204832 | tf_op jit(solution)/shard_map/ppermute | solution.py:493
  113.9 3.1 %shard_map.194 = bf16[384,256]{1,0:T(8,128)(2,1)S(1)} custom-call(s32[2]{0:T(128)S(1)} %pad_add_fusion.place_ref.refs_0_, bf16[2,384,128]{2,1,0:T(8,128)(2,1)S(1)} %get-tuple-element.77.q_ref.refs_1_, bf16[384,384]{1,0:T(8,128)(2,1)S(1)} %get-tuple-element.78.later_ref.refs_2_, f32[64,256]{1,0:T(8,128)S(1)} %get-tuple-element.79.refs_3_, ...), custom_call_target="tpu_custom_call" | custom-call | flops 3000000000 | bytes 1000000 | tf_op jit(solution)/shard_map/pallas_call | solution.py:379
  117.1 10.7 %all_to_all.15.parts_ref = bf16[8,48,256]{2,1,0:T(8,128)(2,1)S(1)} all-to-all(bf16[8,48,256]{2,1,0:T(8,128)(2,1)S(1)} %bitcast.15), channel_id=1, replica_groups=mesh['sp'=16,'fs'=4,'tp_0'=4,'tp_1'=2] {'tp_0','tp_1'}, dimensions={0} | all-to-all | bytes 393216 | tf_op jit(solution)/shard_map/all_to_all | solution.py:527
  127.8 3.8 %shard_map.195 = bf16[48,2048]{1,0:T(8,128)(2,1)} custom-call(s32[2]{0:T(128)S(1)} %pad_add_fusion.place_ref.refs_0_, bf16[8,48,256]{2,1,0:T(8,128)(2,1)S(1)} %all_to_all.15.parts_ref, bf16[4,256,2048]{2,1,0:T(8,128)(2,1)} %all-to-all-done.1.mine_ref, bf16[4,256,2048]{2,1,0:T(8,128)(2,1)S(1)} %collective-permute-done.16.other_ref), custom_call_target="tpu_custom_call" | custom-call | flops 1000000000 | bytes 10000000 | tf_op jit(solution)/shard_map/pallas_call | solution.py:528
  (16 shorter events, 0.1 us)
Async XLA Ops:
  2.0 16.6 %all-to-all-start = ((bf16[4,48,2048]{2,1,0:T(8,128)(2,1)}), bf16[4,48,2048]{2,1,0:T(8,128)(2,1)S(1)}, u32[]{:S(2)}, u32[]{:S(2)}) async-start(bf16[4,48,2048]{2,1,0:T(8,128)(2,1)} %shard_map.181), calls=%async_computation | async-start | bytes 1572864 | tf_op jit(solution)/shard_map/all_to_all | solution.py:430
  18.6 4.2 %collective-permute-start = (bf16[192,2048]{1,0:T(8,128)(2,1)S(1)}, bf16[192,2048]{1,0:T(8,128)(2,1)S(1)}, u32[]{:S(2)}, u32[]{:S(2)}) collective-permute-start(bf16[192,2048]{1,0:T(8,128)(2,1)S(1)} %bitcast.13), channel_id=1, source_target_pairs={{0,1},{1,0},{2,3},{3,2},{4,5},{5,4},{6,7},{7,6},{8,9},{9,8},{10,11... | collective-permute-start | bytes 2359304 | tf_op jit(solution)/shard_map/ppermute | solution.py:464
  25.0 76.5 %all-to-all-start.1 = ((bf16[4,256,2048]{2,1,0:T(8,128)(2,1)}), bf16[4,256,2048]{2,1,0:T(8,128)(2,1)}, u32[]{:S(2)}, u32[]{:S(2)}) async-start(bf16[4,256,2048]{2,1,0:T(8,128)(2,1)} %broadcast_in_dim.6), calls=%async_computation.1 | async-start | bytes 8388608 | tf_op jit(solution)/shard_map/all_to_all | solution.py:484
  29.9 4.8 %collective-permute-start.9 = (bf16[400,256]{1,0:T(8,128)(2,1)S(1)}, bf16[400,256]{1,0:T(8,128)(2,1)S(1)}, u32[]{:S(2)}, u32[]{:S(2)}) collective-permute-start(bf16[400,256]{1,0:T(8,128)(2,1)S(1)} %get-tuple-element.80.payload_ref), channel_id=1, source_target_pairs={{0,480},{32,0},{64,32},{96,64},{128,96},{160,128},{192,160},{1,481... | collective-permute-start | bytes 614408 | tf_op jit(solution)/shard_map/ppermute | solution.py:496
  30.6 10.2 %collective-permute-start.1 = (bf16[400,256]{1,0:T(8,128)(2,1)S(1)}, bf16[400,256]{1,0:T(8,128)(2,1)S(1)}, u32[]{:S(2)}, u32[]{:S(2)}) collective-permute-start(bf16[400,256]{1,0:T(8,128)(2,1)S(1)} %get-tuple-element.80.payload_ref), channel_id=1, source_target_pairs={{0,32},{32,64},{64,96},{96,128},{128,160},{160,192},{192,224},{224... | collective-permute-start | bytes 614408 | tf_op jit(solution)/shard_map/ppermute | solution.py:493
  34.7 10.0 %collective-permute-start.10 = (bf16[400,256]{1,0:T(8,128)(2,1)S(1)}, bf16[400,256]{1,0:T(8,128)(2,1)S(1)}, u32[]{:S(2)}, u32[]{:S(2)}) collective-permute-start(bf16[400,256]{1,0:T(8,128)(2,1)S(1)} %collective-permute-done.9.refs_5_), channel_id=1, source_target_pairs={{480,448},{0,480},{32,0},{64,32},{96,64},{128,96},{160,128},{481,4... | collective-permute-start | bytes 614408 | tf_op jit(solution)/shard_map/ppermute | solution.py:496
  40.8 9.5 %collective-permute-start.2 = (bf16[400,256]{1,0:T(8,128)(2,1)S(1)}, bf16[400,256]{1,0:T(8,128)(2,1)S(1)}, u32[]{:S(2)}, u32[]{:S(2)}) collective-permute-start(bf16[400,256]{1,0:T(8,128)(2,1)S(1)} %collective-permute-done.1.refs_4_), channel_id=1, source_target_pairs={{32,64},{64,96},{96,128},{128,160},{160,192},{192,224},{224,256},{... | collective-permute-start | bytes 614408 | tf_op jit(solution)/shard_map/ppermute | solution.py:493
  44.7 9.4 %collective-permute-start.11 = (bf16[400,256]{1,0:T(8,128)(2,1)S(1)}, bf16[400,256]{1,0:T(8,128)(2,1)S(1)}, u32[]{:S(2)}, u32[]{:S(2)}) collective-permute-start(bf16[400,256]{1,0:T(8,128)(2,1)S(1)} %collective-permute-done.10.refs_5_), channel_id=1, source_target_pairs={{448,416},{480,448},{0,480},{32,0},{64,32},{96,64},{128,96},{449,4... | collective-permute-start | bytes 614408 | tf_op jit(solution)/shard_map/ppermute | solution.py:496
  50.3 8.9 %collective-permute-start.3 = (bf16[400,256]{1,0:T(8,128)(2,1)S(1)}, bf16[400,256]{1,0:T(8,128)(2,1)S(1)}, u32[]{:S(2)}, u32[]{:S(2)}) collective-permute-start(bf16[400,256]{1,0:T(8,128)(2,1)S(1)} %collective-permute-done.2.refs_4_), channel_id=1, source_target_pairs={{64,96},{96,128},{128,160},{160,192},{192,224},{224,256},{256,288}... | collective-permute-start | bytes 614408 | tf_op jit(solution)/shard_map/ppermute | solution.py:493
  54.1 8.9 %collective-permute-start.12 = (bf16[400,256]{1,0:T(8,128)(2,1)S(1)}, bf16[400,256]{1,0:T(8,128)(2,1)S(1)}, u32[]{:S(2)}, u32[]{:S(2)}) collective-permute-start(bf16[400,256]{1,0:T(8,128)(2,1)S(1)} %collective-permute-done.11.refs_5_), channel_id=1, source_target_pairs={{416,384},{448,416},{480,448},{0,480},{32,0},{64,32},{96,64},{417,... | collective-permute-start | bytes 614408 | tf_op jit(solution)/shard_map/ppermute | solution.py:496
  59.1 9.0 %collective-permute-start.4 = (bf16[400,256]{1,0:T(8,128)(2,1)S(1)}, bf16[400,256]{1,0:T(8,128)(2,1)S(1)}, u32[]{:S(2)}, u32[]{:S(2)}) collective-permute-start(bf16[400,256]{1,0:T(8,128)(2,1)S(1)} %collective-permute-done.3.refs_4_), channel_id=1, source_target_pairs={{96,128},{128,160},{160,192},{192,224},{224,256},{256,288},{288,32... | collective-permute-start | bytes 614408 | tf_op jit(solution)/shard_map/ppermute | solution.py:493
  63.0 11.1 %collective-permute-start.13 = (bf16[400,256]{1,0:T(8,128)(2,1)S(1)}, bf16[400,256]{1,0:T(8,128)(2,1)S(1)}, u32[]{:S(2)}, u32[]{:S(2)}) collective-permute-start(bf16[400,256]{1,0:T(8,128)(2,1)S(1)} %collective-permute-done.12.refs_5_), channel_id=1, source_target_pairs={{384,352},{416,384},{448,416},{480,448},{0,480},{32,0},{64,32},{38... | collective-permute-start | bytes 614408 | tf_op jit(solution)/shard_map/ppermute | solution.py:496
  68.1 9.2 %collective-permute-start.5 = (bf16[400,256]{1,0:T(8,128)(2,1)S(1)}, bf16[400,256]{1,0:T(8,128)(2,1)S(1)}, u32[]{:S(2)}, u32[]{:S(2)}) collective-permute-start(bf16[400,256]{1,0:T(8,128)(2,1)S(1)} %collective-permute-done.4.refs_4_), channel_id=1, source_target_pairs={{128,160},{160,192},{192,224},{224,256},{256,288},{288,320},{320,3... | collective-permute-start | bytes 614408 | tf_op jit(solution)/shard_map/ppermute | solution.py:493
  74.1 9.1 %collective-permute-start.14 = (bf16[400,256]{1,0:T(8,128)(2,1)S(1)}, bf16[400,256]{1,0:T(8,128)(2,1)S(1)}, u32[]{:S(2)}, u32[]{:S(2)}) collective-permute-start(bf16[400,256]{1,0:T(8,128)(2,1)S(1)} %collective-permute-done.13.refs_5_), channel_id=1, source_target_pairs={{352,320},{384,352},{416,384},{448,416},{480,448},{0,480},{32,0},{... | collective-permute-start | bytes 614408 | tf_op jit(solution)/shard_map/ppermute | solution.py:496
  77.3 10.3 %collective-permute-start.6 = (bf16[400,256]{1,0:T(8,128)(2,1)S(1)}, bf16[400,256]{1,0:T(8,128)(2,1)S(1)}, u32[]{:S(2)}, u32[]{:S(2)}) collective-permute-start(bf16[400,256]{1,0:T(8,128)(2,1)S(1)} %collective-permute-done.5.refs_4_), channel_id=1, source_target_pairs={{160,192},{192,224},{224,256},{256,288},{288,320},{320,352},{352,3... | collective-permute-start | bytes 614408 | tf_op jit(solution)/shard_map/ppermute | solution.py:493
  83.2 9.6 %collective-permute-start.15 = (bf16[400,256]{1,0:T(8,128)(2,1)S(1)}, bf16[400,256]{1,0:T(8,128)(2,1)S(1)}, u32[]{:S(2)}, u32[]{:S(2)}) collective-permute-start(bf16[400,256]{1,0:T(8,128)(2,1)S(1)} %collective-permute-done.14.refs_5_), channel_id=1, source_target_pairs={{320,288},{352,320},{384,352},{416,384},{448,416},{480,448},{0,480... | collective-permute-start | bytes 614408 | tf_op jit(solution)/shard_map/ppermute | solution.py:496
  87.6 8.9 %collective-permute-start.7 = (bf16[400,256]{1,0:T(8,128)(2,1)S(1)}, bf16[400,256]{1,0:T(8,128)(2,1)S(1)}, u32[]{:S(2)}, u32[]{:S(2)}) collective-permute-start(bf16[400,256]{1,0:T(8,128)(2,1)S(1)} %collective-permute-done.6.refs_4_), channel_id=1, source_target_pairs={{192,224},{224,256},{256,288},{288,320},{320,352},{352,384},{384,4... | collective-permute-start | bytes 614408 | tf_op jit(solution)/shard_map/ppermute | solution.py:493
  96.5 3.2 %copy-start = (f32[128]{0:T(128)S(1)}, f32[128]{0:T(128)}, u32[]{:S(2)}) copy-start(f32[128]{0:T(128)} %param.35) | copy-start | bytes 1540
  101.4 26.3 %collective-permute-start.16 = (bf16[4,256,2048]{2,1,0:T(8,128)(2,1)}, bf16[4,256,2048]{2,1,0:T(8,128)(2,1)S(1)}, u32[]{:S(2)}, u32[]{:S(2)}) collective-permute-start(bf16[4,256,2048]{2,1,0:T(8,128)(2,1)} %all-to-all-done.1.mine_ref), channel_id=1, source_target_pairs={{0,1},{1,0},{2,3},{3,2},{4,5},{5,4},{6,7},{7,6},{8,9},{9,8},{10,11... | collective-permute-start | bytes 12582920 | tf_op jit(solution)/shard_map/ppermute | solution.py:516
  103.4 10.6 %collective-permute-start.8 = (bf16[400,256]{1,0:T(8,128)(2,1)S(1)}, bf16[400,256]{1,0:T(8,128)(2,1)S(1)}, u32[]{:S(2)}, u32[]{:S(2)}) collective-permute-start(bf16[400,256]{1,0:T(8,128)(2,1)S(1)} %collective-permute-done.7.refs_4_), channel_id=1, source_target_pairs={{224,256},{256,288},{288,320},{320,352},{352,384},{384,416},{416,4... | collective-permute-start | bytes 614408 | tf_op jit(solution)/shard_map/ppermute | solution.py:493
